TPU v7x, 32 devices: a whole 2x2x4 slice. The times are simulated.
32 devices in a mesh: sp: 16 (over z, y, x), tp: 2 (over core).
Axes of the slice: x: 2, y: 2, z: 4, core: 2. Of those that a mesh axis runs over, the one named last changes fastest.
Arguments:
- value_in: bfloat16 [5760, 2048], P('sp', 'tp'), may hold values from -240 to 240
- gate_in: bfloat16 [5760, 2048], P('sp', 'tp'), may hold values from -8 to 8
- taps: float32 [31, 2048], P(None, 'tp'), may hold values from -1 to 1
- norm_gain: float32 [2048], P('tp'), may hold values from 0.1 to 1.9
- norm_bias: float32 [2048], P('tp'), may hold values from -3 to 3
- proj_weight: bfloat16 [2048, 4096], P('tp', 'sp'), may hold values from -0.125 to 0.125
- out_grad: bfloat16 [5760, 4096], P('sp'), may hold values from -6 to 6
Outputs:
- value_grad: bfloat16 [5760, 2048], P('sp', 'tp')
- gate_grad: bfloat16 [5760, 2048], P('sp', 'tp')
- tap_grad: float32 [31, 2048], P(None, 'tp')
- gain_grad: float32 [2048], P('tp')
- bias_grad: float32 [2048], P('tp')
- weight_grad: float32 [2048, 4096], P('tp', 'sp')
All inputs are finite; a program needn't handle non-finite values.
Results may differ from a plain program's by a relative error of at most 0.0051.
Values may be sent and summed in bfloat16 or wider, within the bound.
No kernel may reach another device: no remote copies, remote signals or barrier semaphores. Data moves between devices by JAX's collectives and lax.ppermute only.
A program may use at most 64 MiB of HBM per device.

v0:
```python
import jax
import jax.numpy as jnp
from jax import lax
from jax.sharding import PartitionSpec as P


def padded_2(cells, sides, width):
    for axis, dim in sides:
        count = lax.axis_size(axis)
        ends = count - 1
        head = lax.slice_in_dim(cells, 0, width, axis=dim)
        tail = lax.slice_in_dim(cells, cells.shape[dim] - width, cells.shape[dim], axis=dim)
        cells = jnp.concatenate(
            [
                lax.ppermute(tail, axis, [(i, (i + 1) % count) for i in range(ends)]),
                cells,
                lax.ppermute(head, axis, [((i + 1) % count, i) for i in range(ends)]),
            ],
            axis=dim,
        )
    return cells


def on_device(value_in, gate_in, taps, norm_gain, norm_bias, proj_weight, out_grad):
    f32 = jnp.float32
    rows = value_in.shape[0]
    local_width = value_in.shape[1]
    span = taps.shape[0]
    half = span // 2
    width_all = local_width * lax.axis_size("tp")
    gate_sig = jax.nn.sigmoid(gate_in.astype(f32))
    value_f = value_in.astype(f32)
    mixed = (value_f * gate_sig).astype(jnp.bfloat16)
    padded = padded_2(mixed, (("sp", 0),), half).astype(f32)
    conv = jnp.zeros((rows, local_width), f32)
    for k in range(span):
        conv = conv + taps[k] * padded[k : k + rows]
    mean = lax.psum(jnp.sum(conv, axis=1), "tp") / width_all
    centred = conv - mean[:, None]
    spread = lax.psum(jnp.sum(centred * centred, axis=1), "tp") / width_all
    inv = lax.rsqrt(spread + 1e-06)
    normed = centred * inv[:, None]
    pre = normed * norm_gain + norm_bias
    act = jax.nn.silu(pre).astype(jnp.bfloat16)
    act_grad = lax.dot_general(
        out_grad,
        lax.all_gather(proj_weight, "sp", axis=1, tiled=True),
        (((1,), (1,)), ((), ())),
        preferred_element_type=f32,
    )
    sig_pre = jax.nn.sigmoid(pre)
    pre_grad = act_grad * sig_pre * (1.0 + pre * (1.0 - sig_pre))
    normed_grad = pre_grad * norm_gain
    first, second = lax.psum(
        (jnp.sum(normed_grad, axis=1), jnp.sum(normed_grad * normed, axis=1)), "tp"
    )
    conv_grad = inv[:, None] * (
        normed_grad - first[:, None] / width_all - normed * second[:, None] / width_all
    )
    extended = padded_2(conv_grad, (("sp", 0),), half)
    mixed_grad = jnp.zeros((rows, local_width), f32)
    for k in range(span):
        mixed_grad = mixed_grad + taps[k] * extended[2 * half - k : 2 * half - k + rows]
    tap_local = jnp.stack([jnp.sum(conv_grad * padded[k : k + rows], axis=0) for k in range(span)])
    gain_local = jnp.sum(pre_grad * normed, axis=0)
    bias_local = jnp.sum(pre_grad, axis=0)
    tap_grad, gain_grad, bias_grad = lax.psum((tap_local, gain_local, bias_local), "sp")
    value_grad = (mixed_grad * gate_sig).astype(jnp.bfloat16)
    gate_grad = (mixed_grad * value_f * gate_sig * (1.0 - gate_sig)).astype(jnp.bfloat16)
    column_grads = lax.all_to_all(out_grad, "sp", split_axis=1, concat_axis=0, tiled=True)
    weight_grad = lax.dot_general(
        lax.all_gather(act, "sp", axis=0, tiled=True),
        column_grads,
        (((0,), (0,)), ((), ())),
        preferred_element_type=f32,
    )
    return (value_grad, gate_grad, tap_grad, gain_grad, bias_grad, weight_grad)


def solution(mesh):
    return jax.shard_map(
        on_device,
        mesh=mesh,
        in_specs=(
            P("sp", "tp"),
            P("sp", "tp"),
            P(None, "tp"),
            P("tp"),
            P("tp"),
            P("tp", "sp"),
            P("sp", None),
        ),
        out_specs=(P("sp", "tp"), P("sp", "tp"), P(None, "tp"), P("tp"), P("tp"), P("tp", "sp")),
        check_vma=False,
    )
```

profile of v0, /device:TPU:0, one launch (start us, length us, event | category | flops | bytes accessed | tf_op | source)
XLA Modules:
  0.0 476.7 jit_solution(5827107920566509336)
XLA Ops:
  7.2 0.0 copy-start.2
  7.2 0.0 all-gather.3.cloned.1.call-start
  7.2 0.7 all-gather.3.cloned.1.call-update
  7.9 0.0 all-gather.5.cloned.1.call-start
  8.0 1.8 fusion
  9.7 4.9 %collective-permute-start = (bf16[15,1024]{1,0:T(8,128)(2,1)S(1)}, bf16[15,1024]{1,0:T(8,128)(2,1)S(1)}, u32[]{:S(2)}, u32[]{:S(2)}) collective-permute-start(bf16[15,1024]{1,0:T(8,128)(2,1)S(1)} %get-tuple-element.53), channel_id=1, source_target_pairs={{0,2},{2,4},{4,6},{6,8},{8,10},{10,12},{12,14},{14,16},{16,18},{18... | collective-permute-start | bytes 92168 | tf_op jit(solution)/shard_map/ppermute | solution.py:15
  14.6 1.3 collective-permute-start.1
  15.9 0.0 copy-done.2
  15.9 0.1 fusion.96
  16.0 0.2 collective-permute-done
  16.2 4.2 collective-permute-done.1
  20.4 0.2 maximum_convert_fusion
  20.7 6.9 %fusion.93 = (f32[360]{0:T(512)S(1)}, f32[360,1024]{1,0:T(8,128)S(1)}) fusion(f32[390,1024]{1,0:T(8,128)S(1)} %maximum_convert_fusion, f32[1024]{0:T(1024)S(1)} %bitcast.133, f32[1024]{0:T(1024)S(1)} %bitcast.135, f32[1024]{0:T(1024)S(1)} %bitcast.77, f32[1024]{0:T(1024)S(1)} %bitcast.79, f32[1024]{0:T(1024)S(1)} %bitcast.81, f32[1024]{0:T(1024)S(1)} %bitcast.83, ...), kind=kLoop, calls=%fused_computation.197 | loop fusion | flops 22855320 | bytes 47314336 | tf_op jit(solution)/shard_map/reduce_sum | solution.py:38
  27.5 0.0 copy-start
  27.5 0.0 copy-start.3
  27.6 0.0 copy-start.4
  27.6 2.6 psum.49
  30.2 0.3 multiply_reduce_fusion.33
  30.5 2.5 psum.50
  32.9 115.0 %all-gather.3.cloned.1.call-done = bf16[1024,4096]{1,0:T(8,128)(2,1)} async-done(((bf16[1024,256]{1,0:T(8,128)(2,1)}), bf16[1024,4096]{1,0:T(8,128)(2,1)}) %all-gather.3.cloned.1.call-update) | async-done | bytes 8388624 | tf_op jit(solution)/shard_map/all_gather | solution.py:47
  147.9 0.0 copy-done.3
  147.9 0.0 copy-done.4
  147.9 10.2 %multiply_reduce_fusion = (f32[1024]{0:T(1024)}, f32[360]{0:T(512)S(1)}, f32[360]{0:T(512)S(1)}, f32[1024]{0:T(1024)}, bf16[360,1024]{1,0:T(8,128)(2,1)}, /*index=5*/f32[360,1024]{1,0:T(8,128)}) fusion(f32[360,1024]{1,0:T(8,128)S(1)} %get-tuple-element.49, f32[360]{0:T(512)S(1)} %add_rsqrt_fusion, f32[360]{0:T(512)S(1)} %broadcast_multiply_fusion.1, ...), kind=kOutput, calls=%fused_computation.150 | convolution fusion | flops 3027637760 | bytes 15046272 | tf_op jit(solution)/shard_map/dot_general | solution.py:45
  158.2 0.0 copy-done
  158.2 0.0 all-gather.5.cloned.1.call-update
  158.2 3.6 copy.17
  161.8 4.5 all-to-all-start
  166.3 0.0 all-reduce.4.cloned.1.call-start
  166.3 2.5 all-reduce.1
  168.8 5.5 %multiply_reduce_fusion.1 = (f32[1024]{0:T(1024)S(1)}, f32[1024]{0:T(1024)S(1)}, f32[1024]{0:T(1024)S(1)}, f32[1024]{0:T(1024)S(1)}, f32[1024]{0:T(1024)S(1)}, /...) fusion(f32[390,1024]{1,0:T(8,128)S(1)} %maximum_convert_fusion,, ...), kind=kLoop, calls=%fused_computation.151 | loop fusion | flops 16201728 | bytes 31049344 | tf_op jit(solution)/shard_map/reduce_sum | solution.py:64
  174.3 1.3 collective-permute-start.2
  175.6 4.5 collective-permute-start.3
  180.2 3.1 multiply_reduce_fusion.2
  183.2 4.1 stack.127
  187.3 0.0 all-reduce.4.cloned.1.call-update
  187.3 91.1 %all-reduce = (f32[1024]{0:T(1024)}, f32[1024]{0:T(1024)}) all-reduce(f32[1024]{0:T(1024)} %get-tuple-element.37, f32[1024]{0:T(1024)} %get-tuple-element.40), channel_id=1, replica_groups=mesh['sp'=16,'tp'=2] {'sp'}, use_global_device_ids=true, to_apply=%region_41.42 | all-reduce | flops 2048 | bytes 16384 | tf_op jit(solution)/shard_map/psum | solution.py:67
  278.4 0.0 copy-start.1
  278.4 0.0 collective-permute-done.2
  278.4 0.0 collective-permute-done.3
  278.4 8.8 %fusion.3 = (bf16[360,1024]{1,0:T(8,128)(2,1)}, f32[360,1024]{1,0:T(8,128)S(1)}) fusion(bf16[360,1024]{1,0:T(8,128)(2,1)} %param.7, bf16[360,1024]{1,0:T(8,128)(2,1)} %param.8, f32[360,1024]{1,0:T(8,128)S(1)} %get-tuple-element.45, f32[15,1024]{1,0:T(8,128)S(1)} %collective-permute-done.3, f32[1024]{0:T(1024)S(1)} %bitcast.134, f32[1024]{0:T(1024)S(1)} %bitcast.136, ...), kind=kLoop, calls=%fused_computation.34 | loop fusion | flops 37232640 | bytes 5410816 | tf_op jit(solution)/shard_map/convert_element_type | solution.py:69
  287.2 0.0 copy-done.1
  287.2 1.3 multiply_convert_fusion.1
  288.5 0.0 all-to-all-done
  288.5 70.6 %all-gather.5.cloned.1.call-done = bf16[5760,1024]{1,0:T(8,128)(2,1)} async-done(((bf16[360,1024]{1,0:T(8,128)(2,1)}), bf16[5760,1024]{1,0:T(8,128)(2,1)}) %all-gather.5.cloned.1.call-update) | async-done | bytes 11796496 | tf_op jit(solution)/shard_map/all_gather | solution.py:72
  359.1 9.5 %fusion.98 = f32[1024,256]{1,0:T(8,128)} fusion(bf16[5760,1024]{1,0:T(8,128)(2,1)} %all-gather.5.cloned.1.call-done, bf16[5760,256]{1,0:T(8,128)(2,1)} %bitcast.63), kind=kOutput, calls=%fused_computation.202 | convolution fusion | flops 3019898880 | bytes 15794176 | tf_op jit(solution)/shard_map/dot_general | solution.py:71
  368.6 100.0 %all-reduce.4.cloned.1.call-done = f32[31,1024]{1,0:T(8,128)} async-done(((f32[31,1024]{1,0:T(8,128)}), f32[31,1024]{1,0:T(8,128)}) %all-reduce.4.cloned.1.call-update) | async-done | bytes 126992 | tf_op jit(solution)/shard_map/psum | solution.py:67
  468.6 1.6 copy.19
  (6 shorter events, 0.1 us)
Async XLA Ops:
  7.2 8.8 %copy-start.2 = (f32[31,1024]{1,0:T(8,128)S(1)}, f32[31,1024]{1,0:T(8,128)}, u32[]{:S(2)}) copy-start(f32[31,1024]{1,0:T(8,128)} %param.9) | copy-start | bytes 380932
  7.2 140.8 %all-gather.3.cloned.1.call-start = ((), (), s32[]{:S(2)}) async-start(), calls=%async_computation.1 | async-start | bytes 8912896 | tf_op jit(solution)/shard_map/all_gather | solution.py:47
  7.9 351.2 %all-gather.5.cloned.1.call-start = ((), (), s32[]{:S(2)}) async-start(), calls=%async_computation.3 | async-start | bytes 12533760 | tf_op jit(solution)/shard_map/all_gather | solution.py:72
  9.7 6.5 %collective-permute-start = (bf16[15,1024]{1,0:T(8,128)(2,1)S(1)}, bf16[15,1024]{1,0:T(8,128)(2,1)S(1)}, u32[]{:S(2)}, u32[]{:S(2)}) collective-permute-start(bf16[15,1024]{1,0:T(8,128)(2,1)S(1)} %get-tuple-element.53), channel_id=1, source_target_pairs={{0,2},{2,4},{4,6},{6,8},{8,10},{10,12},{12,14},{14,16},{16,18},{18... | collective-permute-start | bytes 92168 | tf_op jit(solution)/shard_map/ppermute | solution.py:15
  14.6 5.8 %collective-permute-start.1 = (bf16[15,1024]{1,0:T(8,128)(2,1)S(1)}, bf16[15,1024]{1,0:T(8,128)(2,1)S(1)}, u32[]{:S(2)}, u32[]{:S(2)}) collective-permute-start(bf16[15,1024]{1,0:T(8,128)(2,1)S(1)} %get-tuple-element.54), channel_id=1, source_target_pairs={{2,0},{4,2},{6,4},{8,6},{10,8},{12,10},{14,12},{16,14},{18,16},{20... | collective-permute-start | bytes 92168 | tf_op jit(solution)/shard_map/ppermute | solution.py:17
  27.5 130.6 %copy-start = (f32[360,1024]{1,0:T(8,128)}, f32[360,1024]{1,0:T(8,128)S(1)}, u32[]{:S(2)}) copy-start(f32[360,1024]{1,0:T(8,128)S(1)} %get-tuple-element.49) | copy-start | bytes 4423684
  27.5 120.4 %copy-start.3 = (f32[1024]{0:T(1024)S(1)}, f32[1024]{0:T(1024)}, u32[]{:S(2)}) copy-start(f32[1024]{0:T(1024)} %param.10) | copy-start | bytes 12292
  27.6 120.4 %copy-start.4 = (f32[1024]{0:T(1024)S(1)}, f32[1024]{0:T(1024)}, u32[]{:S(2)}) copy-start(f32[1024]{0:T(1024)} %param.11) | copy-start | bytes 12292
  161.8 126.7 %all-to-all-start = ((bf16[360,16,256]{2,0,1:T(8,128)(2,1)}), bf16[360,16,256]{2,0,1:T(8,128)(2,1)}, u32[]{:S(2)}, u32[]{:S(2)}) async-start(bf16[360,16,256]{2,0,1:T(8,128)(2,1)} %bitcast.73), calls=%async_computation | async-start | bytes 5898240 | tf_op jit(solution)/shard_map/all_to_all | solution.py:70
  166.3 302.3 %all-reduce.4.cloned.1.call-start = ((), (), s32[]{:S(2)}) async-start(), calls=%async_computation.2 | async-start | bytes 262144 | tf_op jit(solution)/shard_map/psum | solution.py:67
  174.3 104.1 %collective-permute-start.2 = (f32[15,1024]{1,0:T(8,128)S(1)}, f32[15,1024]{1,0:T(8,128)S(1)}, u32[]{:S(2)}, u32[]{:S(2)}) collective-permute-start(f32[15,1024]{1,0:T(8,128)S(1)} %get-tuple-element.51), channel_id=1, source_target_pairs={{2,0},{4,2},{6,4},{8,6},{10,8},{12,10},{14,12},{16,14},{18,16},{20... | collective-permute-start | bytes 184328 | tf_op jit(solution)/shard_map/ppermute | solution.py:17
  175.6 102.8 %collective-permute-start.3 = (f32[15,1024]{1,0:T(8,128)S(1)}, f32[15,1024]{1,0:T(8,128)S(1)}, u32[]{:S(2)}, u32[]{:S(2)}) collective-permute-start(f32[15,1024]{1,0:T(8,128)S(1)} %get-tuple-element.52), channel_id=1, source_target_pairs={{0,2},{2,4},{4,6},{6,8},{8,10},{10,12},{12,14},{14,16},{16,18},{18... | collective-permute-start | bytes 184328 | tf_op jit(solution)/shard_map/ppermute | solution.py:15
  278.4 8.8 %copy-start.1 = (bf16[360,1024]{1,0:T(8,128)(2,1)S(1)}, bf16[360,1024]{1,0:T(8,128)(2,1)}, u32[]{:S(2)}) copy-start(bf16[360,1024]{1,0:T(8,128)(2,1)} %param.8) | copy-start | bytes 2211844
Sparse Core Ops, SparseCore 0:
  10.7 137.1 all-gather.2
  158.3 200.7 all-gather.4
  365.1 103.3 all-reduce.3
where the time goes:
time: 477 us
  waiting for transfers between devices  291 us (61%)
  blocking collectives  98.6 us (21%)
  other arithmetic  27.7 us (6%)
  matrix products  19.7 us (4%)
  starting transfers between devices  16.6 us (3%)
  between operations  13.9 us (3%)
  local copies, waits for them, and re-layouts  9.41 us (2%)
    all_gather x1, waiting for transfers between devices, on_device(): lax.all_gather(proj_weight, 'sp', axis=1, tiled=True)  115 us
    psum x1, waiting for transfers between devices, on_device(): lax.psum((tap_local, gain_local, bias_local), 'sp')  100 us
    psum x1, blocking collectives, on_device(): lax.psum((tap_local, gain_local, bias_local), 'sp')  91.1 us
    all_gather x1, waiting for transfers between devices, on_device(): lax.all_gather(act, 'sp', axis=0, tiled=True)  70.6 us
    dot_general x1, matrix products, on_device(): lax.dot_general(out_grad, lax.all_gather(proj_weight, 'sp', axis=1, tiled...  10.2 us
  transfers between devices with their start and end apart: 8, of which 5 were waited for; matrix products, arithmetic and copies ran while one was open for 9% of the time, Pallas kernels for 0%

commit v1 on v0

v1 whole, which is shorter than its diff:
```python
import jax
import jax.numpy as jnp
from jax import lax
from jax.sharding import Mesh, PartitionSpec as P


SP = ("far", "near")


def padded_2(cells, axis, width):
    count = lax.axis_size(axis)
    ends = count - 1
    head = lax.slice_in_dim(cells, 0, width, axis=0)
    tail = lax.slice_in_dim(cells, cells.shape[0] - width, cells.shape[0], axis=0)
    return jnp.concatenate(
        [
            lax.ppermute(tail, axis, [(i, (i + 1) % count) for i in range(ends)]),
            cells,
            lax.ppermute(head, axis, [((i + 1) % count, i) for i in range(ends)]),
        ],
        axis=0,
    )


def exchange(blocks, axis):
    return lax.all_to_all(blocks, axis, split_axis=0, concat_axis=0)


def spread_out(block, axis):
    count = lax.axis_size(axis)
    return exchange(jnp.broadcast_to(block[None], (count,) + block.shape), axis)


def sum_over(parts, axis):
    count = lax.axis_size(axis)
    rows, width = parts.shape
    each = -(-rows // count)
    blocks = jnp.pad(parts, ((0, each * count - rows), (0, 0))).reshape(count, each, width)
    mine = jnp.sum(exchange(blocks, axis), axis=0)
    return spread_out(mine, axis).reshape(each * count, width)[:rows]


def paired(count):
    return count & (count - 1) == 0


def partner(index, step, count):
    return index ^ step if paired(count) else (index + step) % count


def send(block, axis, step):
    count = lax.axis_size(axis)
    return lax.ppermute(block, axis, [(i, partner(i, step, count)) for i in range(count)])


def fetch(block, axis, step):
    count = lax.axis_size(axis)
    return lax.ppermute(block, axis, [(partner(i, step, count), i) for i in range(count)])


def plane_columns(out_grad, cols):
    far, near, tp = (lax.axis_size(a) for a in ("far", "near", "tp"))
    rows = out_grad.shape[0]
    shared = far % tp == 0
    piece = far // tp if shared else far
    base = lax.axis_index("tp") * piece if shared else 0
    me = lax.axis_index("far")
    blocks = []
    for n in range(near):
        for k in range(piece):
            start = (partner(me, base + k, far) * near + n) * cols
            blocks.append(lax.dynamic_slice_in_dim(out_grad, start, cols, axis=1))
    blocks = jnp.stack(blocks).reshape(near, piece, rows, cols)
    got = exchange(blocks, "near")
    got = got.transpose(1, 0, 2, 3)
    if shared:
        got = spread_out(got, "tp")
    return got.reshape(far, near * rows, cols)


def on_device(value_in, gate_in, taps, norm_gain, norm_bias, proj_weight, out_grad):
    f32 = jnp.float32
    bf16 = jnp.bfloat16
    rows, local_width = value_in.shape
    span = taps.shape[0]
    half = span // 2
    width_all = local_width * lax.axis_size("tp")
    cols = proj_weight.shape[1]
    far = lax.axis_size("far")
    near = lax.axis_size("near")

    fetched = [fetch(proj_weight, "far", d) for d in reversed(range(1, far))]
    weight_far = jnp.stack([proj_weight] + fetched[::-1])
    grads = plane_columns(out_grad, cols)

    gate_sig = jax.nn.sigmoid(gate_in.astype(f32))
    value_f = value_in.astype(f32)
    mixed = (value_f * gate_sig).astype(bf16)
    padded = padded_2(mixed, SP, half).astype(f32)
    conv = jnp.zeros((rows, local_width), f32)
    for k in range(span):
        conv = conv + taps[k] * padded[k : k + rows]
    mean = lax.psum(jnp.sum(conv, axis=1), "tp") / width_all
    centred = conv - mean[:, None]
    spread = lax.psum(jnp.sum(centred * centred, axis=1), "tp") / width_all
    inv = lax.rsqrt(spread + 1e-06)
    normed = centred * inv[:, None]
    pre = normed * norm_gain + norm_bias
    act = jax.nn.silu(pre).astype(bf16)

    act, grads = lax.optimization_barrier((act, grads))
    act_near = spread_out(act, "near")

    partial = lax.dot_general(
        grads, weight_far, (((0, 2), (0, 2)), ((), ())), preferred_element_type=f32
    ).astype(bf16).reshape(near, rows, local_width)
    grad_parts = exchange(partial, "near")
    act_grad = jnp.sum(grad_parts.astype(f32), axis=0)

    act_near = act_near.reshape(near * rows, local_width)
    weight_grad = None
    for d in reversed(range(far)):
        part = lax.dot_general(
            act_near, grads[d], (((0,), (0,)), ((), ())), preferred_element_type=f32
        )
        part = part.astype(bf16) if d else part
        if d:
            part = send(part, "far", d).astype(f32)
        weight_grad = part if weight_grad is None else weight_grad + part

    sig_pre = jax.nn.sigmoid(pre)
    pre_grad = act_grad * sig_pre * (1.0 + pre * (1.0 - sig_pre))
    normed_grad = pre_grad * norm_gain
    first, second = lax.psum(
        (jnp.sum(normed_grad, axis=1), jnp.sum(normed_grad * normed, axis=1)), "tp"
    )
    conv_grad = inv[:, None] * (
        normed_grad - first[:, None] / width_all - normed * second[:, None] / width_all
    )
    extended = padded_2(conv_grad, SP, half)
    sums = [jnp.sum(conv_grad * padded[k : k + rows], axis=0) for k in range(span)]
    sums.append(jnp.sum(pre_grad * normed, axis=0))
    sums.append(jnp.sum(pre_grad, axis=0))
    totals = sum_over(jnp.stack(sums), SP)
    mixed_grad = jnp.zeros((rows, local_width), f32)
    for k in range(span):
        mixed_grad = mixed_grad + taps[k] * extended[2 * half - k : 2 * half - k + rows]
    value_grad = (mixed_grad * gate_sig).astype(bf16)
    gate_grad = (mixed_grad * value_f * gate_sig * (1.0 - gate_sig)).astype(bf16)
    return (value_grad, gate_grad, totals[:span], totals[span], totals[span + 1], weight_grad)


def solution(mesh):
    count, tp = mesh.shape["sp"], mesh.shape["tp"]
    near = max(d for d in range(1, count + 1) if count % d == 0 and d * d <= count)
    grid = Mesh(mesh.devices.reshape(count // near, near, tp), ("far", "near", "tp"))
    return jax.shard_map(
        on_device,
        mesh=grid,
        in_specs=(
            P(SP, "tp"),
            P(SP, "tp"),
            P(None, "tp"),
            P("tp"),
            P("tp"),
            P("tp", SP),
            P(SP, None),
        ),
        out_specs=(P(SP, "tp"), P(SP, "tp"), P(None, "tp"), P("tp"), P("tp"), P("tp", SP)),
        check_vma=False,
    )
```

time: 477 us -> 256 us (0.54)
  waiting for transfers between devices: 291 us -> 105 us
  blocking collectives: 98.6 us -> 14.6 us
  starting transfers between devices: 16.6 us -> 56.3 us
  between operations: 13.9 us -> 1.34 us
  local copies, waits for them, and re-layouts: 9.41 us -> 20.6 us
  other arithmetic: 27.7 us -> 34.4 us
    all_gather x2 -> x0, waiting for transfers between devices: 186 us -> none  [the longest x1 115 us: on_device(): lax.all_gather(proj_weight, 'sp', axis=1, tiled=True)]
    psum x1 -> x0, waiting for transfers between devices: 100 us -> none  [on_device(): lax.psum((tap_local, gain_local, bias_local), 'sp')]
    psum x1 -> x0, blocking collectives: 91.1 us -> none  [on_device(): lax.psum((tap_local, gain_local, bias_local), 'sp')]
    all_to_all x1 -> x5, waiting for transfers between devices: 0.01 us -> 68.8 us  [exchange(): return lax.all_to_all(blocks, axis, split_axis=0, concat_axis=0)]
    ppermute x0 -> x6, waiting for transfers between devices: none -> 35.8 us  [the longest x3 35.8 us: fetch(): lax.ppermute(block, axis, [(partner(i, step, count), i) for i in range(co...]
    all_to_all x1 -> x5, starting transfers between devices: 4.5 us -> 25.3 us  [exchange(): return lax.all_to_all(blocks, axis, split_axis=0, concat_axis=0)]
    ppermute x0 -> x6, starting transfers between devices: none -> 19 us  [the longest x3 13.6 us: send(): lax.ppermute(block, axis, [(i, partner(i, step, count)) for i in range(co...]
    unnamed x11 -> x73, local copies, waits for them, and re-layouts: 1.59 us -> 11.4 us
  transfers between devices with their start and end apart: 8 -> 15, of which waited for: 5 -> 6; matrix products, arithmetic and copies ran while one was open for 9% -> 22% of each run, Pallas kernels for 0% -> 0%
where the time goes in v1:
time: 256 us; the launch traced here: 255 us
  waiting for transfers between devices  105 us (41%)
  starting transfers between devices  56.3 us (22%)
  other arithmetic  34.4 us (13%)
  matrix products  22.9 us (9%)
  local copies, waits for them, and re-layouts  20.6 us (8%)
  blocking collectives  14.6 us (6%)
    all_to_all x5, waiting for transfers between devices, exchange(): return lax.all_to_all(blocks, axis, split_axis=0, concat_axis=0)  68.8 us
    ppermute x3, waiting for transfers between devices, fetch(): lax.ppermute(block, axis, [(partner(i, step, count), i) for i in range(co...  35.8 us
    all_to_all x5, starting transfers between devices, exchange(): return lax.all_to_all(blocks, axis, split_axis=0, concat_axis=0)  25.3 us
    dot_general x4, matrix products, on_device(): lax.dot_general(act_near, grads[d], (((0,), (0,)), ((), ())), preferred_e...  16.1 us
    ppermute x3, starting transfers between devices, send(): lax.ppermute(block, axis, [(i, partner(i, step, count)) for i in range(co...  13.6 us
    unnamed x73, local copies, waits for them, and re-layouts  11.4 us
    ppermute x2, starting transfers between devices, padded_2(): lax.ppermute(tail, axis, [(i, (i + 1) % count) for i in range(ends)])  9.42 us
    convert_element_type x1, other arithmetic, on_device(): (mixed_grad * value_f * gate_sig * (1.0 - gate_sig)).astype(bf16)  8.84 us
  transfers between devices with their start and end apart: 15, of which 6 were waited for; matrix products, arithmetic and copies ran while one was open for 22% of the time, Pallas kernels for 0%

profile of v1, /device:TPU:0, one launch (start us, length us, event | category | flops | bytes accessed | tf_op | source)
XLA Modules:
  0.0 254.7 jit_solution(8580267400963913671)
XLA Ops:
  0.6 1.8 fusion.7
  2.4 4.9 %collective-permute-start = (bf16[15,1024]{1,0:T(8,128)(2,1)S(1)}, bf16[15,1024]{1,0:T(8,128)(2,1)S(1)}, u32[]{:S(2)}, u32[]{:S(2)}) collective-permute-start(bf16[15,1024]{1,0:T(8,128)(2,1)S(1)} %get-tuple-element.55), channel_id=1, source_target_pairs={{0,2},{2,4},{4,6},{6,8},{8,10},{10,12},{12,14},{14,16},{16,18},{18... | collective-permute-start | bytes 92168 | tf_op jit(solution)/shard_map/ppermute | solution.py:17
  7.3 1.3 collective-permute-start.1
  8.6 1.6 bitcast_dynamic-update-slice_fusion.7
  10.2 1.6 bitcast_dynamic-update-slice_fusion.6
  11.9 1.6 bitcast_dynamic-update-slice_fusion.5
  13.5 1.6 bitcast_dynamic-update-slice_fusion.4
  15.1 1.6 bitcast_dynamic-update-slice_fusion.3
  16.7 1.6 bitcast_dynamic-update-slice_fusion.2
  18.3 1.6 bitcast_dynamic-update-slice_fusion.1
  19.9 1.6 bitcast_dynamic-update-slice_fusion
  21.5 5.0 %all-to-all-start = ((bf16[4,2,360,256]{3,2,1,0:T(8,128)(2,1)}), bf16[4,2,360,256]{3,2,1,0:T(8,128)(2,1)}, u32[]{:S(2)}, u32[]{:S(2)}) async-start(bf16[4,2,360,256]{3,2,1,0:T(8,128)(2,1)} %bitcast.39), calls=%async_computation | async-start | bytes 2949120 | tf_op jit(solution)/shard_map/all_to_all | solution.py:26
  27.0 6.9 %fusion.112 = (f32[360]{0:T(512)S(1)}, f32[360,1024]{1,0:T(8,128)S(1)}) fusion(f32[390,1024]{1,0:T(8,128)S(1)} %maximum_convert_fusion, f32[1024]{0:T(1024)S(1)} %bitcast.176, f32[1024]{0:T(1024)S(1)} %bitcast.178, f32[1024]{0:T(1024)S(1)} %bitcast.120, f32[1024]{0:T(1024)S(1)} %bitcast.122, f32[1024]{0:T(1024)S(1)} %bitcast.124, f32[1024]{0:T(1024)S(1)} %bitcast.126, ...), kind=kLoop, calls=%fused_computation.227 | loop fusion | flops 22855320 | bytes 47314336 | tf_op jit(solution)/shard_map/reduce_sum | solution.py:103
  34.1 2.5 psum.28
  36.9 2.5 psum.29
  39.4 1.4 multiply_convert_fusion.1
  40.8 4.9 %all-to-all-done = bf16[4,2,360,256]{3,2,1,0:T(8,128)(2,1)} async-done(((bf16[4,2,360,256]{3,2,1,0:T(8,128)(2,1)}), bf16[4,2,360,256]{3,2,1,0:T(8,128)(2,1)}, u32[]{:S(2)}, u32[]{:S(2)}) %all-to-all-start) | async-done | bytes 1474592 | tf_op jit(solution)/shard_map/all_to_all | solution.py:26
  45.7 1.5 copy.13
  47.4 7.2 %all_to_all.30 = bf16[2,2,4,360,256]{4,3,2,1,0:T(8,128)(2,1)} all-to-all(bf16[2,2,4,360,256]{4,3,2,1,0:T(8,128)(2,1)S(1)} %broadcast_in_dim.6), channel_id=1, replica_groups=mesh['far'=4,'near'=4,'tp'=2] {'tp'}, dimensions={0} | all-to-all | bytes 5898240 | tf_op jit(solution)/shard_map/all_to_all | solution.py:26
  54.6 2.0 broadcast_in_dim.8
  56.6 4.6 %all-to-all-start.5 = ((bf16[4,360,1024]{2,1,0:T(8,128)(2,1)}), bf16[4,360,1024]{2,1,0:T(8,128)(2,1)}, u32[]{:S(2)}, u32[]{:S(2)}) async-start(bf16[4,360,1024]{2,1,0:T(8,128)(2,1)} %broadcast_in_dim.8), calls=%async_computation.5 | async-start | bytes 5898240 | tf_op jit(solution)/shard_map/all_to_all | solution.py:26
  61.3 2.8 %collective-permute-start.2 = (bf16[1024,256]{1,0:T(8,128)(2,1)}, bf16[1024,256]{1,0:T(8,128)(2,1)S(1)}, u32[]{:S(2)}, u32[]{:S(2)}) collective-permute-start(bf16[1024,256]{1,0:T(8,128)(2,1)} %param.12), channel_id=1, source_target_pairs={{8,0},{0,8},{24,16},{16,24},{9,1},{1,9},{25,17},{17,25},{10,2},{2,... | collective-permute-start | bytes 1572872 | tf_op jit(solution)/shard_map/ppermute | solution.py:58
  64.0 2.6 %collective-permute-start.3 = (bf16[1024,256]{1,0:T(8,128)(2,1)}, bf16[1024,256]{1,0:T(8,128)(2,1)S(1)}, u32[]{:S(2)}, u32[]{:S(2)}) collective-permute-start(bf16[1024,256]{1,0:T(8,128)(2,1)} %param.12), channel_id=1, source_target_pairs={{16,0},{24,8},{0,16},{8,24},{17,1},{25,9},{1,17},{9,25},{18,2},{26... | collective-permute-start | bytes 1572872 | tf_op jit(solution)/shard_map/ppermute | solution.py:58
  66.6 20.5 %collective-permute-done.2 = bf16[1024,256]{1,0:T(8,128)(2,1)S(1)} collective-permute-done((bf16[1024,256]{1,0:T(8,128)(2,1)}, bf16[1024,256]{1,0:T(8,128)(2,1)S(1)}, u32[]{:S(2)}, u32[]{:S(2)}) %collective-permute-start.2) | collective-permute-done | bytes 524320 | tf_op jit(solution)/shard_map/ppermute | solution.py:58
  87.1 15.3 %collective-permute-done.3 = bf16[1024,256]{1,0:T(8,128)(2,1)S(1)} collective-permute-done((bf16[1024,256]{1,0:T(8,128)(2,1)}, bf16[1024,256]{1,0:T(8,128)(2,1)S(1)}, u32[]{:S(2)}, u32[]{:S(2)}) %collective-permute-start.3) | collective-permute-done | bytes 524320 | tf_op jit(solution)/shard_map/ppermute | solution.py:58
  102.4 6.8 %bitcast_convert_fusion = bf16[1440,1024]{1,0:T(8,128)(2,1)} fusion(bf16[4,1440,256]{2,1,0:T(8,128)(2,1)} %bitcast.112, bf16[1,1024,256]{2,1,0:T(8,128)(2,1)S(1)} %bitcast.218, bf16[1,1024,256]{2,1,0:T(8,128)(2,1)S(1)} %bitcast.217, bf16[1,1024,256]{2,1,0:T(8,128)(2,1)S(1)} %bitcast.216, bf16[1,1024,256]{2,1,0:T(8,128)(2,1)} %bitcast.215), kind=kOutput, calls=%fused_computation.28 | convolution fusion | flops 3024519168 | bytes 7995392 | tf_op jit(solution)/shard_map/dot_general | solution.py:114
  109.3 4.9 %all-to-all-start.2 = ((bf16[4,360,1024]{2,1,0:T(8,128)(2,1)}), bf16[4,360,1024]{2,1,0:T(8,128)(2,1)}, u32[]{:S(2)}, u32[]{:S(2)}) async-start(bf16[4,360,1024]{2,1,0:T(8,128)(2,1)} %bitcast.117), calls=%async_computation.2 | async-start | bytes 5898240 | tf_op jit(solution)/shard_map/all_to_all | solution.py:26
  114.1 3.8 %convolution_convert_fusion.2 = bf16[1024,256]{1,0:T(8,128)(2,1)} fusion(bf16[1440,1024]{1,0:T(8,128)(2,1)} %bitcast.83, bf16[4,1440,256]{2,1,0:T(8,128)(2,1)} %bitcast.113), kind=kOutput, calls=%fused_computation.202 | convolution fusion | flops 755236864 | bytes 4210688 | tf_op jit(solution)/shard_map/dot_general | solution.py:123
  118.0 3.8 %convolution_convert_fusion.1 = bf16[1024,256]{1,0:T(8,128)(2,1)} fusion(bf16[1440,1024]{1,0:T(8,128)(2,1)} %bitcast.83, bf16[4,1440,256]{2,1,0:T(8,128)(2,1)} %bitcast.114), kind=kOutput, calls=%fused_computation.201 | convolution fusion | flops 755236864 | bytes 4210688 | tf_op jit(solution)/shard_map/dot_general | solution.py:123
  121.8 24.7 %all-to-all-done.2 = bf16[4,360,1024]{2,1,0:T(8,128)(2,1)} async-done(((bf16[4,360,1024]{2,1,0:T(8,128)(2,1)}), bf16[4,360,1024]{2,1,0:T(8,128)(2,1)}, u32[]{:S(2)}, u32[]{:S(2)}) %all-to-all-start.2) | async-done | bytes 2949152 | tf_op jit(solution)/shard_map/all_to_all | solution.py:26
  146.5 2.6 %convert_reduce_fusion = f32[360,1024]{1,0:T(8,128)S(1)} fusion(bf16[4,360,1024]{2,1,0:T(8,128)(2,1)} %all-to-all-done.2), kind=kLoop, calls=%fused_computation.29 | loop fusion | flops 2580480 | bytes 4423680 | tf_op jit(solution)/shard_map/reduce_sum | solution.py:118
  149.1 2.8 %multiply_reduce_fusion = (f32[1024]{0:T(1024)}, f32[360]{0:T(512)S(1)}, f32[360]{0:T(512)S(1)}, f32[1024]{0:T(1024)}, f32[360,1024]{1,0:T(8,128)}) fusion(f32[360,1024]{1,0:T(8,128)S(1)} %get-tuple-element.52, f32[360]{0:T(512)S(1)} %add_rsqrt_fusion, f32[360]{0:T(512)S(1)} %broadcast_multiply_fusion.1, f32[1024]{0:T(1024)S(1)} %copy-done.25, ...), kind=kLoop, calls=%fused_computation.157 | loop fusion | flops 7001392 | bytes 4445824 | tf_op jit(solution)/shard_map/reduce_sum | solution.py:142
  151.9 2.4 all-reduce.1
  154.3 5.9 %multiply_reduce_fusion.1 = (f32[1024]{0:T(1024)S(1)}, f32[1024]{0:T(1024)S(1)}, f32[1024]{0:T(1024)S(1)}, f32[1024]{0:T(1024)S(1)}, f32[1024]{0:T(1024)S(1)}, /...) fusion(f32[390,1024]{1,0:T(8,128)S(1)} %maximum_convert_fusion,, ...), kind=kLoop, calls=%fused_computation.158 | loop fusion | flops 16201728 | bytes 31049344 | tf_op jit(solution)/shard_map/reduce_sum | solution.py:141
  160.2 2.4 multiply_reduce_fusion.2
  163.3 1.3 collective-permute-start.5
  164.6 4.5 %collective-permute-start.6 = (f32[15,1024]{1,0:T(8,128)S(1)}, f32[15,1024]{1,0:T(8,128)S(1)}, u32[]{:S(2)}, u32[]{:S(2)}) collective-permute-start(f32[15,1024]{1,0:T(8,128)S(1)} %get-tuple-element.54), channel_id=1, source_target_pairs={{0,2},{2,4},{4,6},{6,8},{8,10},{10,12},{12,14},{14,16},{16,18},{18... | collective-permute-start | bytes 184328 | tf_op jit(solution)/shard_map/ppermute | solution.py:17
  169.2 3.9 %convolution_convert_fusion = bf16[1024,256]{1,0:T(8,128)(2,1)} fusion(bf16[1440,1024]{1,0:T(8,128)(2,1)} %bitcast.83, bf16[4,1440,256]{2,1,0:T(8,128)(2,1)} %bitcast.115), kind=kOutput, calls=%fused_computation.200 | convolution fusion | flops 755236864 | bytes 4210688 | tf_op jit(solution)/shard_map/dot_general | solution.py:123
  173.2 13.0 %collective-permute-start.7 = (bf16[1024,256]{1,0:T(8,128)(2,1)}, bf16[1024,256]{1,0:T(8,128)(2,1)}, u32[]{:S(2)}, u32[]{:S(2)}) collective-permute-start(bf16[1024,256]{1,0:T(8,128)(2,1)} %convolution_convert_fusion.2), channel_id=1, source_target_pairs={{0,24},{8,16},{16,8},{24,0},{1,25},{9,17},{17,9},{25,1},{2,26},{10... | collective-permute-start | bytes 1572872 | tf_op jit(solution)/shard_map/ppermute | solution.py:53
  187.1 0.8 reshape.42
  187.9 6.6 %all-to-all-start.3 = ((f32[16,3,1024]{2,1,0:T(4,128)}), f32[16,3,1024]{2,1,0:T(4,128)S(1)}, u32[]{:S(2)}, u32[]{:S(2)}) async-start(f32[16,3,1024]{2,1,0:T(4,128)} %reshape.42), calls=%async_computation.3 | async-start | bytes 524288 | tf_op jit(solution)/shard_map/all_to_all | solution.py:26
  194.6 8.8 %fusion.10 = (bf16[360,1024]{1,0:T(8,128)(2,1)}, f32[360,1024]{1,0:T(8,128)S(1)}) fusion(bf16[360,1024]{1,0:T(8,128)(2,1)S(1)} %copy-done.3, bf16[360,1024]{1,0:T(8,128)(2,1)S(1)} %copy-done.2, f32[360,1024]{1,0:T(8,128)S(1)} %copy-done.1, f32[15,1024]{1,0:T(8,128)S(1)} %collective-permute-done.6, f32[1024]{0:T(1024)} %bitcast.177, f32[1024]{0:T(1024)} %bitcast.179, ...), kind=kLoop, calls=%fused_computation.42 | loop fusion | flops 37232640 | bytes 5410816 | tf_op jit(solution)/shard_map/convert_element_type | solution.py:149
  203.5 1.3 multiply_convert_fusion
  204.7 34.1 %all-to-all-done.3 = f32[16,3,1024]{2,1,0:T(4,128)S(1)} async-done(((f32[16,3,1024]{2,1,0:T(4,128)}), f32[16,3,1024]{2,1,0:T(4,128)S(1)}, u32[]{:S(2)}, u32[]{:S(2)}) %all-to-all-start.3) | async-done | bytes 196640 | tf_op jit(solution)/shard_map/all_to_all | solution.py:26
  238.9 0.7 broadcast_in_dim.7
  239.6 4.2 %all-to-all-start.4 = ((f32[16,3,1024]{2,1,0:T(4,128)}), f32[16,3,1024]{2,1,0:T(4,128)S(1)}, u32[]{:S(2)}, u32[]{:S(2)}) async-start(f32[16,3,1024]{2,1,0:T(4,128)} %broadcast_in_dim.7), calls=%async_computation.4 | async-start | bytes 524288 | tf_op jit(solution)/shard_map/all_to_all | solution.py:26
  243.8 4.5 %add_add_fusion = f32[1024,256]{1,0:T(8,128)} fusion(bf16[1024,256]{1,0:T(8,128)(2,1)} %collective-permute-done.9, bf16[1024,256]{1,0:T(8,128)(2,1)} %collective-permute-done.8, bf16[1024,256]{1,0:T(8,128)(2,1)} %collective-permute-done.7, bf16[1440,1024]{1,0:T(8,128)(2,1)} %bitcast.83, bf16[4,1440,256]{2,1,0:T(8,128)(2,1)} %bitcast.116), kind=kOutput, calls=%fused_computation.204 | convolution fusion | flops 756547584 | bytes 6307840 | tf_op jit(solution)/shard_map/dot_general | solution.py:123
  248.3 5.1 %all-to-all-done.4 = f32[16,3,1024]{2,1,0:T(4,128)S(1)} async-done(((f32[16,3,1024]{2,1,0:T(4,128)}), f32[16,3,1024]{2,1,0:T(4,128)S(1)}, u32[]{:S(2)}, u32[]{:S(2)}) %all-to-all-start.4) | async-done | bytes 196640 | tf_op jit(solution)/shard_map/all_to_all | solution.py:26
  (95 shorter events, 3.9 us)
Async XLA Ops:
  2.4 24.4 %collective-permute-start = (bf16[15,1024]{1,0:T(8,128)(2,1)S(1)}, bf16[15,1024]{1,0:T(8,128)(2,1)S(1)}, u32[]{:S(2)}, u32[]{:S(2)}) collective-permute-start(bf16[15,1024]{1,0:T(8,128)(2,1)S(1)} %get-tuple-element.55), channel_id=1, source_target_pairs={{0,2},{2,4},{4,6},{6,8},{8,10},{10,12},{12,14},{14,16},{16,18},{18... | collective-permute-start | bytes 92168 | tf_op jit(solution)/shard_map/ppermute | solution.py:17
  7.3 19.5 %collective-permute-start.1 = (bf16[15,1024]{1,0:T(8,128)(2,1)S(1)}, bf16[15,1024]{1,0:T(8,128)(2,1)S(1)}, u32[]{:S(2)}, u32[]{:S(2)}) collective-permute-start(bf16[15,1024]{1,0:T(8,128)(2,1)S(1)} %get-tuple-element.56), channel_id=1, source_target_pairs={{2,0},{4,2},{6,4},{8,6},{10,8},{12,10},{14,12},{16,14},{18,16},{20... | collective-permute-start | bytes 92168 | tf_op jit(solution)/shard_map/ppermute | solution.py:19
  21.5 5.0 %copy-start.5 = (f32[31,1024]{1,0:T(8,128)S(1)}, f32[31,1024]{1,0:T(8,128)}, u32[]{:S(2)}) copy-start(f32[31,1024]{1,0:T(8,128)} %param.9) | copy-start | bytes 380932
  21.5 24.2 %all-to-all-start = ((bf16[4,2,360,256]{3,2,1,0:T(8,128)(2,1)}), bf16[4,2,360,256]{3,2,1,0:T(8,128)(2,1)}, u32[]{:S(2)}, u32[]{:S(2)}) async-start(bf16[4,2,360,256]{3,2,1,0:T(8,128)(2,1)} %bitcast.39), calls=%async_computation | async-start | bytes 2949120 | tf_op jit(solution)/shard_map/all_to_all | solution.py:26
  26.6 7.4 %copy-start.6 = (f32[1,1024]{1,0:T(1,128)}, f32[1,1024]{1,0:T(1,128)S(1)}, u32[]{:S(2)}) copy-start(f32[1,1024]{1,0:T(1,128)S(1)} %get-tuple-element.71) | copy-start | bytes 12292
  26.6 7.4 %copy-start.7 = (f32[1,1024]{1,0:T(1,128)}, f32[1,1024]{1,0:T(1,128)S(1)}, u32[]{:S(2)}) copy-start(f32[1,1024]{1,0:T(1,128)S(1)} %get-tuple-element.72) | copy-start | bytes 12292
  26.6 7.4 %copy-start.8 = (f32[1,1024]{1,0:T(1,128)}, f32[1,1024]{1,0:T(1,128)S(1)}, u32[]{:S(2)}) copy-start(f32[1,1024]{1,0:T(1,128)S(1)} %get-tuple-element.73) | copy-start | bytes 12292
  26.6 7.4 %copy-start.9 = (f32[1,1024]{1,0:T(1,128)}, f32[1,1024]{1,0:T(1,128)S(1)}, u32[]{:S(2)}) copy-start(f32[1,1024]{1,0:T(1,128)S(1)} %get-tuple-element.74) | copy-start | bytes 12292
  26.6 7.4 %copy-start.10 = (f32[1,1024]{1,0:T(1,128)}, f32[1,1024]{1,0:T(1,128)S(1)}, u32[]{:S(2)}) copy-start(f32[1,1024]{1,0:T(1,128)S(1)} %get-tuple-element.75) | copy-start | bytes 12292
  26.6 7.4 %copy-start.11 = (f32[1,1024]{1,0:T(1,128)}, f32[1,1024]{1,0:T(1,128)S(1)}, u32[]{:S(2)}) copy-start(f32[1,1024]{1,0:T(1,128)S(1)} %get-tuple-element.76) | copy-start | bytes 12292
  26.6 7.4 %copy-start.12 = (f32[1,1024]{1,0:T(1,128)}, f32[1,1024]{1,0:T(1,128)S(1)}, u32[]{:S(2)}) copy-start(f32[1,1024]{1,0:T(1,128)S(1)} %get-tuple-element.77) | copy-start | bytes 12292
  26.7 7.3 %copy-start.13 = (f32[1,1024]{1,0:T(1,128)}, f32[1,1024]{1,0:T(1,128)S(1)}, u32[]{:S(2)}) copy-start(f32[1,1024]{1,0:T(1,128)S(1)} %get-tuple-element.78) | copy-start | bytes 12292
  26.7 7.3 %copy-start.14 = (f32[1,1024]{1,0:T(1,128)}, f32[1,1024]{1,0:T(1,128)S(1)}, u32[]{:S(2)}) copy-start(f32[1,1024]{1,0:T(1,128)S(1)} %get-tuple-element.79) | copy-start | bytes 12292
  26.7 7.3 %copy-start.15 = (f32[1,1024]{1,0:T(1,128)}, f32[1,1024]{1,0:T(1,128)S(1)}, u32[]{:S(2)}) copy-start(f32[1,1024]{1,0:T(1,128)S(1)} %get-tuple-element.80) | copy-start | bytes 12292
  26.7 7.3 %copy-start.16 = (f32[1,1024]{1,0:T(1,128)}, f32[1,1024]{1,0:T(1,128)S(1)}, u32[]{:S(2)}) copy-start(f32[1,1024]{1,0:T(1,128)S(1)} %get-tuple-element.81) | copy-start | bytes 12292
  26.7 7.3 %copy-start.17 = (f32[1,1024]{1,0:T(1,128)}, f32[1,1024]{1,0:T(1,128)S(1)}, u32[]{:S(2)}) copy-start(f32[1,1024]{1,0:T(1,128)S(1)} %get-tuple-element.82) | copy-start | bytes 12292
  26.7 7.3 %copy-start.18 = (f32[1,1024]{1,0:T(1,128)}, f32[1,1024]{1,0:T(1,128)S(1)}, u32[]{:S(2)}) copy-start(f32[1,1024]{1,0:T(1,128)S(1)} %get-tuple-element.83) | copy-start | bytes 12292
  26.7 7.3 %copy-start.19 = (f32[1,1024]{1,0:T(1,128)}, f32[1,1024]{1,0:T(1,128)S(1)}, u32[]{:S(2)}) copy-start(f32[1,1024]{1,0:T(1,128)S(1)} %get-tuple-element.84) | copy-start | bytes 12292
  26.7 7.3 %copy-start.20 = (f32[1,1024]{1,0:T(1,128)}, f32[1,1024]{1,0:T(1,128)S(1)}, u32[]{:S(2)}) copy-start(f32[1,1024]{1,0:T(1,128)S(1)} %get-tuple-element.85) | copy-start | bytes 12292
  26.8 7.3 %copy-start.21 = (f32[1,1024]{1,0:T(1,128)}, f32[1,1024]{1,0:T(1,128)S(1)}, u32[]{:S(2)}) copy-start(f32[1,1024]{1,0:T(1,128)S(1)} %get-tuple-element.86) | copy-start | bytes 12292
  26.8 7.3 %copy-start.22 = (f32[1,1024]{1,0:T(1,128)}, f32[1,1024]{1,0:T(1,128)S(1)}, u32[]{:S(2)}) copy-start(f32[1,1024]{1,0:T(1,128)S(1)} %get-tuple-element.87) | copy-start | bytes 12292
  26.8 7.3 %copy-start.23 = (f32[1,1024]{1,0:T(1,128)}, f32[1,1024]{1,0:T(1,128)S(1)}, u32[]{:S(2)}) copy-start(f32[1,1024]{1,0:T(1,128)S(1)} %get-tuple-element.88) | copy-start | bytes 12292
  26.8 7.3 %copy-start.24 = (f32[1,1024]{1,0:T(1,128)}, f32[1,1024]{1,0:T(1,128)S(1)}, u32[]{:S(2)}) copy-start(f32[1,1024]{1,0:T(1,128)S(1)} %get-tuple-element.89) | copy-start | bytes 12292
  34.1 5.3 %copy-start.25 = (f32[1024]{0:T(1024)S(1)}, f32[1024]{0:T(1024)}, u32[]{:S(2)}) copy-start(f32[1024]{0:T(1024)} %param.10) | copy-start | bytes 12292
  34.1 5.3 %copy-start.30 = (f32[1024]{0:T(1024)S(1)}, f32[1024]{0:T(1024)}, u32[]{:S(2)}) copy-start(f32[1024]{0:T(1024)} %param.11) | copy-start | bytes 12292
  47.4 7.2 %copy-start.4 = (bf16[360,1024]{1,0:T(8,128)(2,1)S(1)}, bf16[360,1024]{1,0:T(8,128)(2,1)}, u32[]{:S(2)}) copy-start(bf16[360,1024]{1,0:T(8,128)(2,1)} %multiply_convert_fusion.1) | copy-start | bytes 2211844
  56.6 52.6 %all-to-all-start.5 = ((bf16[4,360,1024]{2,1,0:T(8,128)(2,1)}), bf16[4,360,1024]{2,1,0:T(8,128)(2,1)}, u32[]{:S(2)}, u32[]{:S(2)}) async-start(bf16[4,360,1024]{2,1,0:T(8,128)(2,1)} %broadcast_in_dim.8), calls=%async_computation.5 | async-start | bytes 5898240 | tf_op jit(solution)/shard_map/all_to_all | solution.py:26
  61.3 25.9 %collective-permute-start.2 = (bf16[1024,256]{1,0:T(8,128)(2,1)}, bf16[1024,256]{1,0:T(8,128)(2,1)S(1)}, u32[]{:S(2)}, u32[]{:S(2)}) collective-permute-start(bf16[1024,256]{1,0:T(8,128)(2,1)} %param.12), channel_id=1, source_target_pairs={{8,0},{0,8},{24,16},{16,24},{9,1},{1,9},{25,17},{17,25},{10,2},{2,... | collective-permute-start | bytes 1572872 | tf_op jit(solution)/shard_map/ppermute | solution.py:58
  64.0 38.4 %collective-permute-start.3 = (bf16[1024,256]{1,0:T(8,128)(2,1)}, bf16[1024,256]{1,0:T(8,128)(2,1)S(1)}, u32[]{:S(2)}, u32[]{:S(2)}) collective-permute-start(bf16[1024,256]{1,0:T(8,128)(2,1)} %param.12), channel_id=1, source_target_pairs={{16,0},{24,8},{0,16},{8,24},{17,1},{25,9},{1,17},{9,25},{18,2},{26... | collective-permute-start | bytes 1572872 | tf_op jit(solution)/shard_map/ppermute | solution.py:58
  66.6 35.8 %collective-permute-start.4 = (bf16[1024,256]{1,0:T(8,128)(2,1)}, bf16[1024,256]{1,0:T(8,128)(2,1)S(1)}, u32[]{:S(2)}, u32[]{:S(2)}) collective-permute-start(bf16[1024,256]{1,0:T(8,128)(2,1)} %param.12), channel_id=1, source_target_pairs={{24,0},{16,8},{8,16},{0,24},{25,1},{17,9},{9,17},{1,25},{26,2},{18... | collective-permute-start | bytes 1572872 | tf_op jit(solution)/shard_map/ppermute | solution.py:58
  109.3 37.2 %all-to-all-start.2 = ((bf16[4,360,1024]{2,1,0:T(8,128)(2,1)}), bf16[4,360,1024]{2,1,0:T(8,128)(2,1)}, u32[]{:S(2)}, u32[]{:S(2)}) async-start(bf16[4,360,1024]{2,1,0:T(8,128)(2,1)} %bitcast.117), calls=%async_computation.2 | async-start | bytes 5898240 | tf_op jit(solution)/shard_map/all_to_all | solution.py:26
  160.2 2.4 copy-start
  163.3 31.3 %collective-permute-start.5 = (f32[15,1024]{1,0:T(8,128)}, f32[15,1024]{1,0:T(8,128)S(1)}, u32[]{:S(2)}, u32[]{:S(2)}) collective-permute-start(f32[15,1024]{1,0:T(8,128)} %get-tuple-element.53), channel_id=1, source_target_pairs={{2,0},{4,2},{6,4},{8,6},{10,8},{12,10},{14,12},{16,14},{18,16},{20... | collective-permute-start | bytes 184328 | tf_op jit(solution)/shard_map/ppermute | solution.py:19
  164.6 22.2 %copy-start.26 = (f32[1024]{0:T(1024)S(1)}, f32[1024]{0:T(1024)}, u32[]{:S(2)}) copy-start(f32[1024]{0:T(1024)} %get-tuple-element.24) | copy-start | bytes 12292
  164.6 22.2 %copy-start.27 = (f32[1024]{0:T(1024)S(1)}, f32[1024]{0:T(1024)}, u32[]{:S(2)}) copy-start(f32[1024]{0:T(1024)} %get-tuple-element.25) | copy-start | bytes 12292
  164.6 22.2 %copy-start.28 = (f32[1024]{0:T(1024)S(1)}, f32[1024]{0:T(1024)}, u32[]{:S(2)}) copy-start(f32[1024]{0:T(1024)} %get-tuple-element.26) | copy-start | bytes 12292
  164.6 22.2 %copy-start.29 = (f32[1024]{0:T(1024)S(1)}, f32[1024]{0:T(1024)}, u32[]{:S(2)}) copy-start(f32[1024]{0:T(1024)} %get-tuple-element.27) | copy-start | bytes 12292
  164.6 22.2 %copy-start.31 = (f32[1024]{0:T(1024)S(1)}, f32[1024]{0:T(1024)}, u32[]{:S(2)}) copy-start(f32[1024]{0:T(1024)} %get-tuple-element.41) | copy-start | bytes 12292
  164.6 22.2 %copy-start.32 = (f32[1024]{0:T(1024)S(1)}, f32[1024]{0:T(1024)}, u32[]{:S(2)}) copy-start(f32[1024]{0:T(1024)} %get-tuple-element.44) | copy-start | bytes 12292
  164.6 29.9 %collective-permute-start.6 = (f32[15,1024]{1,0:T(8,128)S(1)}, f32[15,1024]{1,0:T(8,128)S(1)}, u32[]{:S(2)}, u32[]{:S(2)}) collective-permute-start(f32[15,1024]{1,0:T(8,128)S(1)} %get-tuple-element.54), channel_id=1, source_target_pairs={{0,2},{2,4},{4,6},{6,8},{8,10},{10,12},{12,14},{14,16},{16,18},{18... | collective-permute-start | bytes 184328 | tf_op jit(solution)/shard_map/ppermute | solution.py:17
  169.2 25.4 %copy-start.2 = (bf16[360,1024]{1,0:T(8,128)(2,1)S(1)}, bf16[360,1024]{1,0:T(8,128)(2,1)}, u32[]{:S(2)}) copy-start(bf16[360,1024]{1,0:T(8,128)(2,1)} %param.8) | copy-start | bytes 2211844
  169.2 25.4 %copy-start.3 = (bf16[360,1024]{1,0:T(8,128)(2,1)S(1)}, bf16[360,1024]{1,0:T(8,128)(2,1)}, u32[]{:S(2)}) copy-start(bf16[360,1024]{1,0:T(8,128)(2,1)} %param.7) | copy-start | bytes 2211844
  173.2 21.4 %copy-start.1 = (f32[360,1024]{1,0:T(8,128)S(1)}, f32[360,1024]{1,0:T(8,128)}, u32[]{:S(2)}) copy-start(f32[360,1024]{1,0:T(8,128)} %copy-done) | copy-start | bytes 4423684
  173.2 70.6 %collective-permute-start.7 = (bf16[1024,256]{1,0:T(8,128)(2,1)}, bf16[1024,256]{1,0:T(8,128)(2,1)}, u32[]{:S(2)}, u32[]{:S(2)}) collective-permute-start(bf16[1024,256]{1,0:T(8,128)(2,1)} %convolution_convert_fusion.2), channel_id=1, source_target_pairs={{0,24},{8,16},{16,8},{24,0},{1,25},{9,17},{17,9},{25,1},{2,26},{10... | collective-permute-start | bytes 1572872 | tf_op jit(solution)/shard_map/ppermute | solution.py:53
  186.2 57.6 %collective-permute-start.8 = (bf16[1024,256]{1,0:T(8,128)(2,1)}, bf16[1024,256]{1,0:T(8,128)(2,1)}, u32[]{:S(2)}, u32[]{:S(2)}) collective-permute-start(bf16[1024,256]{1,0:T(8,128)(2,1)} %convolution_convert_fusion.1), channel_id=1, source_target_pairs={{0,16},{8,24},{16,0},{24,8},{1,17},{9,25},{17,1},{25,9},{2,18},{10... | collective-permute-start | bytes 1572872 | tf_op jit(solution)/shard_map/ppermute | solution.py:53
  186.4 57.4 %collective-permute-start.9 = (bf16[1024,256]{1,0:T(8,128)(2,1)}, bf16[1024,256]{1,0:T(8,128)(2,1)}, u32[]{:S(2)}, u32[]{:S(2)}) collective-permute-start(bf16[1024,256]{1,0:T(8,128)(2,1)} %convolution_convert_fusion), channel_id=1, source_target_pairs={{0,8},{8,0},{16,24},{24,16},{1,9},{9,1},{17,25},{25,17},{2,10},{10... | collective-permute-start | bytes 1572872 | tf_op jit(solution)/shard_map/ppermute | solution.py:53
  187.9 50.9 %all-to-all-start.3 = ((f32[16,3,1024]{2,1,0:T(4,128)}), f32[16,3,1024]{2,1,0:T(4,128)S(1)}, u32[]{:S(2)}, u32[]{:S(2)}) async-start(f32[16,3,1024]{2,1,0:T(4,128)} %reshape.42), calls=%async_computation.3 | async-start | bytes 524288 | tf_op jit(solution)/shard_map/all_to_all | solution.py:26
  239.6 13.7 %all-to-all-start.4 = ((f32[16,3,1024]{2,1,0:T(4,128)}), f32[16,3,1024]{2,1,0:T(4,128)S(1)}, u32[]{:S(2)}, u32[]{:S(2)}) async-start(f32[16,3,1024]{2,1,0:T(4,128)} %broadcast_in_dim.7), calls=%async_computation.4 | async-start | bytes 524288 | tf_op jit(solution)/shard_map/all_to_all | solution.py:26

commit v2 on v1

--- a/solution.py
+++ b/solution.py
@@ -1,6 +1,8 @@
 import jax
 import jax.numpy as jnp
 from jax import lax
+from jax.experimental import pallas as pl
+from jax.experimental.pallas import tpu as pltpu
 from jax.sharding import Mesh, PartitionSpec as P
 
 
@@ -36,7 +38,8 @@
     rows, width = parts.shape
     each = -(-rows // count)
     blocks = jnp.pad(parts, ((0, each * count - rows), (0, 0))).reshape(count, each, width)
-    mine = jnp.sum(exchange(blocks, axis), axis=0)
+    blocks = exchange(blocks, axis)
+    mine = jnp.sum(blocks, axis=0)
     return spread_out(mine, axis).reshape(each * count, width)[:rows]
 
 
@@ -44,38 +47,78 @@
     return count & (count - 1) == 0
 
 
-def partner(index, step, count):
-    return index ^ step if paired(count) else (index + step) % count
-
-
-def send(block, axis, step):
-    count = lax.axis_size(axis)
-    return lax.ppermute(block, axis, [(i, partner(i, step, count)) for i in range(count)])
-
-
-def fetch(block, axis, step):
-    count = lax.axis_size(axis)
-    return lax.ppermute(block, axis, [(partner(i, step, count), i) for i in range(count)])
+def split_of(far, tp):
+    shared = far % tp == 0 and paired(far) and paired(tp)
+    return (far // tp if shared else far), shared
+
+
+def partner(row, core, slot, far, tp):
+    piece, shared = split_of(far, tp)
+    if shared:
+        return row ^ slot ^ (core * piece)
+    return row ^ slot if paired(far) else (row + slot) % far
+
+
+def links(slot):
+    far, tp = lax.axis_size("far"), lax.axis_size("tp")
+    return [
+        (row * tp + core, partner(row, core, slot, far, tp) * tp + core)
+        for row in range(far)
+        for core in range(tp)
+    ]
+
+
+def send(block, slot):
+    return lax.ppermute(block, ("far", "tp"), links(slot))
+
+
+def fetch(block, slot):
+    return lax.ppermute(block, ("far", "tp"), [(b, a) for a, b in links(slot)])
+
+
+def copy_block(places, source, target):
+    target[0] = source[...]
+
+
+def column_blocks(out_grad, places, cols):
+    rows = out_grad.shape[0]
+    if cols % 128:
+        return jnp.stack([lax.dynamic_slice_in_dim(out_grad, p * cols, cols, axis=1) for p in places])
+    count = len(places)
+    return pl.pallas_call(
+        copy_block,
+        grid_spec=pltpu.PrefetchScalarGridSpec(
+            num_scalar_prefetch=1,
+            grid=(count,),
+            in_specs=[pl.BlockSpec((rows, cols), lambda g, p: (0, p[g]))],
+            out_specs=pl.BlockSpec((1, rows, cols), lambda g, p: (g, 0, 0)),
+        ),
+        out_shape=jax.ShapeDtypeStruct((count, rows, cols), out_grad.dtype),
+        name="column_blocks",
+    )(jnp.stack(places), out_grad)
 
 
 def plane_columns(out_grad, cols):
     far, near, tp = (lax.axis_size(a) for a in ("far", "near", "tp"))
     rows = out_grad.shape[0]
-    shared = far % tp == 0
-    piece = far // tp if shared else far
-    base = lax.axis_index("tp") * piece if shared else 0
-    me = lax.axis_index("far")
-    blocks = []
-    for n in range(near):
-        for k in range(piece):
-            start = (partner(me, base + k, far) * near + n) * cols
-            blocks.append(lax.dynamic_slice_in_dim(out_grad, start, cols, axis=1))
-    blocks = jnp.stack(blocks).reshape(near, piece, rows, cols)
+    piece, _ = split_of(far, tp)
+    row, core = lax.axis_index("far"), lax.axis_index("tp")
+    places = [
+        (partner(row, core, k, far, tp) * near + n).astype(jnp.int32)
+        for n in range(near)
+        for k in range(piece)
+    ]
+    blocks = column_blocks(out_grad, places, cols).reshape(near, piece, rows, cols)
     got = exchange(blocks, "near")
-    got = got.transpose(1, 0, 2, 3)
-    if shared:
-        got = spread_out(got, "tp")
-    return got.reshape(far, near * rows, cols)
+    return got.transpose(1, 0, 2, 3).reshape(piece, near * rows, cols)
+
+
+def other_cores(got):
+    tp = lax.axis_size("tp")
+    if not split_of(lax.axis_size("far"), tp)[1]:
+        return got
+    swaps = [[(i, i ^ e) for i in range(tp)] for e in range(1, tp)]
+    return jnp.concatenate([got] + [lax.ppermute(got, "tp", s) for s in swaps])
 
 
 def on_device(value_in, gate_in, taps, norm_gain, norm_bias, proj_weight, out_grad):
@@ -89,9 +132,9 @@
     far = lax.axis_size("far")
     near = lax.axis_size("near")
 
-    fetched = [fetch(proj_weight, "far", d) for d in reversed(range(1, far))]
-    weight_far = jnp.stack([proj_weight] + fetched[::-1])
-    grads = plane_columns(out_grad, cols)
+    fetched = [fetch(proj_weight, d) for d in reversed(range(far))]
+    weight_far = jnp.stack(fetched[::-1])
+    got = plane_columns(out_grad, cols)
 
     gate_sig = jax.nn.sigmoid(gate_in.astype(f32))
     value_f = value_in.astype(f32)
@@ -108,8 +151,9 @@
     pre = normed * norm_gain + norm_bias
     act = jax.nn.silu(pre).astype(bf16)
 
-    act, grads = lax.optimization_barrier((act, grads))
+    act, got = lax.optimization_barrier((act, got))
     act_near = spread_out(act, "near")
+    grads = other_cores(got)
 
     partial = lax.dot_general(
         grads, weight_far, (((0, 2), (0, 2)), ((), ())), preferred_element_type=f32
@@ -122,10 +166,8 @@
     for d in reversed(range(far)):
         part = lax.dot_general(
             act_near, grads[d], (((0,), (0,)), ((), ())), preferred_element_type=f32
-        )
-        part = part.astype(bf16) if d else part
-        if d:
-            part = send(part, "far", d).astype(f32)
+        ).astype(bf16)
+        part = send(part, d).astype(f32)
         weight_grad = part if weight_grad is None else weight_grad + part
 
     sig_pre = jax.nn.sigmoid(pre)

time: 256 us -> 198 us (0.77)
  waiting for transfers between devices: 105 us -> 40.5 us
  starting transfers between devices: 56.3 us -> 74.3 us
  local copies, waits for them, and re-layouts: 20.6 us -> 9.87 us
  blocking collectives: 14.6 us -> 7.38 us
  Pallas kernels: 0 us -> 6.08 us
    all_to_all x5, waiting for transfers between devices: 68.8 us -> 6.4 us  [exchange(): return lax.all_to_all(blocks, axis, split_axis=0, concat_axis=0)]
    unnamed x73 -> x52, local copies, waits for them, and re-layouts: 11.4 us -> 1.27 us
    ppermute x6 -> x9, starting transfers between devices: 19 us -> 28.8 us  [the longest x4 19.8 us: send(): return lax.ppermute(block, ('far', 'tp'), links(slot))]
    all_to_all x5, starting transfers between devices: 25.3 us -> 33.3 us  [exchange(): return lax.all_to_all(blocks, axis, split_axis=0, concat_axis=0)]
    all_to_all x1 -> x0, blocking collectives: 7.2 us -> none  [exchange(): return lax.all_to_all(blocks, axis, split_axis=0, concat_axis=0)]
    pallas_call x0 -> x1, Pallas kernels: none -> 6.08 us  [column_blocks(): pl.pallas_call(copy_block, grid_spec=pltpu.PrefetchScalarGridSpec(num_sca...]
    add x0 -> x1, other arithmetic: none -> 2.73 us  [on_device(): weight_grad = part if weight_grad is None else weight_grad + part]
    ppermute x6 -> x9, waiting for transfers between devices: 35.8 us -> 34.1 us  [the longest x4 34.1 us: fetch(): return lax.ppermute(block, ('far', 'tp'), [(b, a) for a, b in links(slot)])]
  transfers between devices with their start and end apart: 15 -> 18, of which waited for: 6 -> 4; matrix products, arithmetic and copies ran while one was open for 22% -> 30% of each run, Pallas kernels for 0% -> 3%
where the time goes in v2:
time: 198 us; the launch traced here: 197 us
  starting transfers between devices  74.3 us (38%)
  waiting for transfers between devices  40.5 us (20%)
  other arithmetic  36 us (18%)
  matrix products  21.3 us (11%)
  local copies, waits for them, and re-layouts  9.87 us (5%)
  blocking collectives  7.38 us (4%)
  Pallas kernels  6.08 us (3%)
    ppermute x4, waiting for transfers between devices, fetch(): return lax.ppermute(block, ('far', 'tp'), [(b, a) for a, b in links(slot)])  34.1 us
    all_to_all x5, starting transfers between devices, exchange(): return lax.all_to_all(blocks, axis, split_axis=0, concat_axis=0)  33.3 us
    ppermute x4, starting transfers between devices, send(): return lax.ppermute(block, ('far', 'tp'), links(slot))  19.8 us
    dot_general x4, matrix products, on_device(): lax.dot_general(act_near, grads[d], (((0,), (0,)), ((), ())), preferred_e...  15 us
    ppermute x2, starting transfers between devices, padded_2(): lax.ppermute(tail, axis, [(i, (i + 1) % count) for i in range(ends)])  9.55 us
    ppermute x4, starting transfers between devices, fetch(): return lax.ppermute(block, ('far', 'tp'), [(b, a) for a, b in links(slot)])  8.95 us
    convert_element_type x1, other arithmetic, on_device(): (mixed_grad * value_f * gate_sig * (1.0 - gate_sig)).astype(bf16)  8.78 us
    reduce_sum x2, other arithmetic, on_device(): jnp.sum(conv_grad * padded[k:k + rows], axis=0)  7.73 us
  transfers between devices with their start and end apart: 18, of which 4 were waited for; matrix products, arithmetic and copies ran while one was open for 30% of the time, Pallas kernels for 3%

profile of v2, /device:TPU:0, one launch (start us, length us, event | category | flops | bytes accessed | tf_op | source)
XLA Modules:
  0.0 196.7 jit_solution(15105423724981314733)
XLA Ops:
  0.6 1.8 fusion.10
  2.4 4.9 %collective-permute-start = (bf16[15,1024]{1,0:T(8,128)(2,1)S(1)}, bf16[15,1024]{1,0:T(8,128)(2,1)S(1)}, u32[]{:S(2)}, u32[]{:S(2)}) collective-permute-start(bf16[15,1024]{1,0:T(8,128)(2,1)S(1)} %get-tuple-element.55), channel_id=1, source_target_pairs={{0,2},{2,4},{4,6},{6,8},{8,10},{10,12},{12,14},{14,16},{16,18},{18... | collective-permute-start | bytes 92168 | tf_op jit(solution)/shard_map/ppermute | solution.py:19
  7.3 1.3 collective-permute-start.1
  8.6 0.7 stack.152.places
  9.3 6.1 %column_blocks.1 = bf16[8,360,256]{2,1,0:T(8,128)(2,1)} custom-call(s32[8]{0:T(128)} %stack.152.places, bf16[360,4096]{1,0:T(8,128)(2,1)} %source.1), custom_call_target="tpu_custom_call" | custom-call | tf_op jit(solution)/shard_map/column_blocks/pallas_call | solution.py:88
  15.4 5.0 %all-to-all-start = ((bf16[4,2,360,256]{3,2,1,0:T(8,128)(2,1)}), bf16[4,2,360,256]{3,2,1,0:T(8,128)(2,1)}, u32[]{:S(2)}, u32[]{:S(2)}) async-start(bf16[4,2,360,256]{3,2,1,0:T(8,128)(2,1)} %bitcast.101), calls=%async_computation | async-start | bytes 2949120 | tf_op jit(solution)/shard_map/all_to_all | solution.py:28
  20.9 6.9 %fusion.108 = (f32[360]{0:T(512)S(1)}, f32[360,1024]{1,0:T(8,128)S(1)}) fusion(f32[390,1024]{1,0:T(8,128)S(1)} %maximum_convert_fusion, f32[1024]{0:T(1024)S(1)} %bitcast.165, f32[1024]{0:T(1024)S(1)} %bitcast.167, f32[1024]{0:T(1024)S(1)} %bitcast.109, f32[1024]{0:T(1024)S(1)} %bitcast.111, f32[1024]{0:T(1024)S(1)} %bitcast.113, f32[1024]{0:T(1024)S(1)} %bitcast.115, ...), kind=kLoop, calls=%fused_computation.220 | loop fusion | flops 22855320 | bytes 47314336 | tf_op jit(solution)/shard_map/reduce_sum | solution.py:146
  27.9 2.5 %psum.28 = f32[360]{0:T(512)S(1)} all-reduce(f32[360]{0:T(512)S(1)} %get-tuple-element.51), channel_id=1, replica_groups=mesh['far'=4,'near'=4,'tp'=2] {'tp'}, use_global_device_ids=true, to_apply=%region_1.0 | all-reduce | flops 360 | bytes 2880 | tf_op jit(solution)/shard_map/psum | solution.py:146
  30.4 0.3 multiply_reduce_fusion.33
  30.7 2.5 %psum.29 = f32[360]{0:T(512)S(1)} all-reduce(f32[360]{0:T(512)S(1)} %multiply_reduce_fusion.33), channel_id=1, replica_groups=mesh['far'=4,'near'=4,'tp'=2] {'tp'}, use_global_device_ids=true, to_apply=%region_3.0 | all-reduce | flops 360 | bytes 2880 | tf_op jit(solution)/shard_map/psum | solution.py:148
  33.2 1.4 multiply_convert_fusion.1
  34.6 5.0 %all-to-all-done = bf16[4,2,360,256]{3,2,1,0:T(8,128)(2,1)} async-done(((bf16[4,2,360,256]{3,2,1,0:T(8,128)(2,1)}), bf16[4,2,360,256]{3,2,1,0:T(8,128)(2,1)}, u32[]{:S(2)}, u32[]{:S(2)}) %all-to-all-start) | async-done | bytes 1474592 | tf_op jit(solution)/shard_map/all_to_all | solution.py:28
  39.7 2.7 %copy.14 = bf16[2,4,360,256]{3,2,1,0:T(8,128)(2,1)} copy(bf16[2,4,360,256]{3,2,0,1:T(8,128)(2,1)} %bitcast.40) | data formatting | bytes 2949120 | tf_op jit(solution)/shard_map/transpose | solution.py:113
  42.3 1.9 broadcast_in_dim.5
  44.3 4.6 %all-to-all-start.4 = ((bf16[4,360,1024]{2,1,0:T(8,128)(2,1)}), bf16[4,360,1024]{2,1,0:T(8,128)(2,1)}, u32[]{:S(2)}, u32[]{:S(2)}) async-start(bf16[4,360,1024]{2,1,0:T(8,128)(2,1)} %broadcast_in_dim.5), calls=%async_computation.4 | async-start | bytes 5898240 | tf_op jit(solution)/shard_map/all_to_all | solution.py:28
  49.0 1.7 collective-permute-start.3
  50.7 2.7 %collective-permute-start.4 = (bf16[1024,256]{1,0:T(8,128)(2,1)}, bf16[1024,256]{1,0:T(8,128)(2,1)S(1)}, u32[]{:S(2)}, u32[]{:S(2)}) collective-permute-start(bf16[1024,256]{1,0:T(8,128)(2,1)} %param.12), channel_id=1, source_target_pairs={{8,0},{25,1},{0,8},{17,9},{24,16},{9,17},{16,24},{1,25},{10,2},{27... | collective-permute-start | bytes 1572872 | tf_op jit(solution)/shard_map/ppermute | solution.py:76
  53.4 4.5 %collective-permute-start.5 = (bf16[1024,256]{1,0:T(8,128)(2,1)}, bf16[1024,256]{1,0:T(8,128)(2,1)S(1)}, u32[]{:S(2)}, u32[]{:S(2)}) collective-permute-start(bf16[1024,256]{1,0:T(8,128)(2,1)} %param.12), channel_id=1, source_target_pairs={{16,0},{1,1},{24,8},{9,9},{0,16},{17,17},{8,24},{25,25},{18,2},{3,... | collective-permute-start | bytes 1572872 | tf_op jit(solution)/shard_map/ppermute | solution.py:76
  57.9 14.2 %collective-permute-done.4 = bf16[1024,256]{1,0:T(8,128)(2,1)S(1)} collective-permute-done((bf16[1024,256]{1,0:T(8,128)(2,1)}, bf16[1024,256]{1,0:T(8,128)(2,1)S(1)}, u32[]{:S(2)}, u32[]{:S(2)}) %collective-permute-start.4) | collective-permute-done | bytes 524320 | tf_op jit(solution)/shard_map/ppermute | solution.py:76
  72.2 19.9 %collective-permute-done.5 = bf16[1024,256]{1,0:T(8,128)(2,1)S(1)} collective-permute-done((bf16[1024,256]{1,0:T(8,128)(2,1)}, bf16[1024,256]{1,0:T(8,128)(2,1)S(1)}, u32[]{:S(2)}, u32[]{:S(2)}) %collective-permute-start.5) | collective-permute-done | bytes 524320 | tf_op jit(solution)/shard_map/ppermute | solution.py:76
  92.0 1.2 copy-done.24
  93.2 6.3 %bitcast_convert_fusion = bf16[1440,1024]{1,0:T(8,128)(2,1)} fusion(bf16[2,1440,256]{2,1,0:T(8,128)(2,1)S(1)} %collective-permute-done.2, bf16[2,1440,256]{2,1,0:T(8,128)(2,1)} %bitcast.104, bf16[1,1024,256]{2,1,0:T(8,128)(2,1)S(1)} %bitcast.207, bf16[1,1024,256]{2,1,0:T(8,128)(2,1)S(1)} %bitcast.206, bf16[1,1024,256]{2,1,0:T(8,128)(2,1)S(1)} %bitcast.205, ...), kind=kOutput, calls=%fused_computation.28 | convolution fusion | flops 3025993728 | bytes 7995392 | tf_op jit(solution)/shard_map/dot_general | solution.py:158
  99.5 4.6 %all-to-all-start.1 = ((bf16[4,360,1024]{2,1,0:T(8,128)(2,1)}), bf16[4,360,1024]{2,1,0:T(8,128)(2,1)}, u32[]{:S(2)}, u32[]{:S(2)}) async-start(bf16[4,360,1024]{2,1,0:T(8,128)(2,1)} %bitcast.102), calls=%async_computation.1 | async-start | bytes 5898240 | tf_op jit(solution)/shard_map/all_to_all | solution.py:28
  104.2 3.9 %convolution_convert_fusion.2 = bf16[1024,256]{1,0:T(8,128)(2,1)} fusion(bf16[1440,1024]{1,0:T(8,128)(2,1)} %bitcast.83, bf16[2,1440,256]{2,1,0:T(8,128)(2,1)} %copy-done.24), kind=kOutput, calls=%fused_computation.205 | convolution fusion | flops 755236864 | bytes 4210688 | tf_op jit(solution)/shard_map/dot_general | solution.py:167
  108.1 13.9 %collective-permute-start.10 = (bf16[1024,256]{1,0:T(8,128)(2,1)}, bf16[1024,256]{1,0:T(8,128)(2,1)}, u32[]{:S(2)}, u32[]{:S(2)}) collective-permute-start(bf16[1024,256]{1,0:T(8,128)(2,1)} %convolution_convert_fusion.2), channel_id=1, source_target_pairs={{0,16},{1,1},{8,24},{9,9},{16,0},{17,17},{24,8},{25,25},{2,18},{3,... | collective-permute-start | bytes 1572872 | tf_op jit(solution)/shard_map/ppermute | solution.py:72
  122.0 3.7 %convolution_convert_fusion.3 = bf16[1024,256]{1,0:T(8,128)(2,1)} fusion(bf16[1440,1024]{1,0:T(8,128)(2,1)} %bitcast.83, bf16[2,1440,256]{2,1,0:T(8,128)(2,1)S(1)} %copy-done.25), kind=kOutput, calls=%fused_computation.206 | convolution fusion | flops 755236864 | bytes 4210688 | tf_op jit(solution)/shard_map/dot_general | solution.py:167
  125.7 0.5 collective-permute-start.9
  126.3 3.7 %convolution_convert_fusion.1 = bf16[1024,256]{1,0:T(8,128)(2,1)} fusion(bf16[1440,1024]{1,0:T(8,128)(2,1)} %bitcast.83, bf16[2,1440,256]{2,1,0:T(8,128)(2,1)S(1)} %bitcast.105), kind=kOutput, calls=%fused_computation.204 | convolution fusion | flops 755236864 | bytes 4210688 | tf_op jit(solution)/shard_map/dot_general | solution.py:167
  130.0 3.7 %convolution_convert_fusion = bf16[1024,256]{1,0:T(8,128)(2,1)} fusion(bf16[1440,1024]{1,0:T(8,128)(2,1)} %bitcast.83, bf16[2,1440,256]{2,1,0:T(8,128)(2,1)S(1)} %bitcast.106), kind=kOutput, calls=%fused_computation.203 | convolution fusion | flops 755236864 | bytes 4210688 | tf_op jit(solution)/shard_map/dot_general | solution.py:167
  133.6 5.3 %collective-permute-start.12 = (bf16[1024,256]{1,0:T(8,128)(2,1)}, bf16[1024,256]{1,0:T(8,128)(2,1)}, u32[]{:S(2)}, u32[]{:S(2)}) collective-permute-start(bf16[1024,256]{1,0:T(8,128)(2,1)} %convolution_convert_fusion), channel_id=1, source_target_pairs={{0,0},{1,17},{8,8},{9,25},{16,16},{17,1},{24,24},{25,9},{2,2},{3,1... | collective-permute-start | bytes 1572872 | tf_op jit(solution)/shard_map/ppermute | solution.py:72
  139.0 2.6 %convert_reduce_fusion = f32[360,1024]{1,0:T(8,128)S(1)} fusion(bf16[4,360,1024]{2,1,0:T(8,128)(2,1)} %all-to-all-done.1), kind=kLoop, calls=%fused_computation.29 | loop fusion | flops 2580480 | bytes 4423680 | tf_op jit(solution)/shard_map/reduce_sum | solution.py:162
  141.6 2.2 %multiply_reduce_fusion = (f32[1024]{0:T(1024)S(1)}, f32[360]{0:T(512)S(1)}, f32[360]{0:T(512)S(1)}, f32[1024]{0:T(1024)S(1)}, f32[360,1024]{1,0:T(8,128)}) fusion(f32[360,1024]{1,0:T(8,128)S(1)} %get-tuple-element.52, f32[360]{0:T(512)S(1)} %add_rsqrt_fusion, f32[360]{0:T(512)S(1)} %broadcast_multiply_fusion.1, f32[1024]{0:T(1024)S(1)} %copy-done.22, ...), kind=kLoop, calls=%fused_computation.160 | loop fusion | flops 7001392 | bytes 4445824 | tf_op jit(solution)/shard_map/reduce_sum | solution.py:184
  143.8 2.4 %all-reduce.1 = (f32[360]{0:T(512)S(1)}, f32[360]{0:T(512)S(1)}) all-reduce(f32[360]{0:T(512)S(1)} %get-tuple-element.42, f32[360]{0:T(512)S(1)} %get-tuple-element.43), channel_id=1, replica_groups=mesh['far'=4,'near'=4,'tp'=2] {'tp'}, use_global_device_ids=true, to_apply=%region_8.9 | all-reduce | flops 720 | bytes 5760 | tf_op jit(solution)/shard_map/psum | solution.py:176
  146.2 5.3 %multiply_reduce_fusion.1 = (f32[1024]{0:T(1024)S(1)}, f32[1024]{0:T(1024)S(1)}, f32[1024]{0:T(1024)S(1)}, f32[1024]{0:T(1024)S(1)}, f32[1024]{0:T(1024)S(1)}, /...) fusion(f32[390,1024]{1,0:T(8,128)S(1)} %maximum_convert_fusion,, ...), kind=kLoop, calls=%fused_computation.161 | loop fusion | flops 16201728 | bytes 31049344 | tf_op jit(solution)/shard_map/reduce_sum | solution.py:183
  151.6 2.4 %multiply_reduce_fusion.2 = (f32[1024]{0:T(1024)S(1)}, f32[1024]{0:T(1024)S(1)}, f32[1024]{0:T(1024)S(1)}, f32[1024]{0:T(1024)S(1)}, f32[1024]{0:T(1024)S(1)}, /...) fusion(f32[360,1024]{1,0:T(8,128)S(1)} %get-tuple-element.47, ...), kind=kLoop, calls=%fused_computation.162 | loop fusion | flops 9571328 | bytes 20697088 | tf_op jit(solution)/shard_map/reduce_sum | solution.py:183
  154.0 0.3 stack.191
  154.3 0.8 reshape.41
  155.1 12.7 %all-to-all-start.2 = ((f32[16,3,1024]{2,1,0:T(4,128)}), f32[16,3,1024]{2,1,0:T(4,128)S(1)}, u32[]{:S(2)}, u32[]{:S(2)}) async-start(f32[16,3,1024]{2,1,0:T(4,128)} %reshape.41), calls=%async_computation.2 | async-start | bytes 524288 | tf_op jit(solution)/shard_map/all_to_all | solution.py:28
  167.8 1.3 collective-permute-start.7
  169.1 4.7 %collective-permute-start.8 = (f32[15,1024]{1,0:T(8,128)S(1)}, f32[15,1024]{1,0:T(8,128)S(1)}, u32[]{:S(2)}, u32[]{:S(2)}) collective-permute-start(f32[15,1024]{1,0:T(8,128)S(1)} %get-tuple-element.54), channel_id=1, source_target_pairs={{0,2},{2,4},{4,6},{6,8},{8,10},{10,12},{12,14},{14,16},{16,18},{18... | collective-permute-start | bytes 184328 | tf_op jit(solution)/shard_map/ppermute | solution.py:19
  173.8 2.7 %convert_add_fusion = f32[1024,256]{1,0:T(8,128)} fusion(bf16[1024,256]{1,0:T(8,128)(2,1)} %collective-permute-done.12, bf16[1024,256]{1,0:T(8,128)(2,1)} %collective-permute-done.11, bf16[1024,256]{1,0:T(8,128)(2,1)} %collective-permute-done.10, bf16[1024,256]{1,0:T(8,128)(2,1)} %collective-permute-done.9), kind=kLoop, calls=%fused_computation.208 | loop fusion | flops 1835008 | bytes 3145728 | tf_op jit(solution)/shard_map/add | solution.py:171
  176.6 1.4 all-to-all-done.2
  178.0 0.8 broadcast_in_dim.4
  178.8 6.4 %all-to-all-start.3 = ((f32[16,3,1024]{2,1,0:T(4,128)}), f32[16,3,1024]{2,1,0:T(4,128)S(1)}, u32[]{:S(2)}, u32[]{:S(2)}) async-start(f32[16,3,1024]{2,1,0:T(4,128)} %broadcast_in_dim.4), calls=%async_computation.3 | async-start | bytes 524288 | tf_op jit(solution)/shard_map/all_to_all | solution.py:28
  185.3 8.8 %fusion.13 = (bf16[360,1024]{1,0:T(8,128)(2,1)}, f32[360,1024]{1,0:T(8,128)S(1)}) fusion(bf16[360,1024]{1,0:T(8,128)(2,1)S(1)} %copy-done.3, bf16[360,1024]{1,0:T(8,128)(2,1)S(1)} %copy-done.2, f32[360,1024]{1,0:T(8,128)S(1)} %copy-done.1, f32[15,1024]{1,0:T(8,128)S(1)} %collective-permute-done.8, f32[1024]{0:T(1024)} %bitcast.166, f32[1024]{0:T(1024)} %bitcast.168, ...), kind=kLoop, calls=%fused_computation.45 | loop fusion | flops 37232640 | bytes 5410816 | tf_op jit(solution)/shard_map/convert_element_type | solution.py:191
  194.0 1.3 multiply_convert_fusion
  195.4 0.7 slice.604
  196.1 0.6 fusion.111
  (80 shorter events, 0.9 us)
Async XLA Ops:
  2.4 18.2 %collective-permute-start = (bf16[15,1024]{1,0:T(8,128)(2,1)S(1)}, bf16[15,1024]{1,0:T(8,128)(2,1)S(1)}, u32[]{:S(2)}, u32[]{:S(2)}) collective-permute-start(bf16[15,1024]{1,0:T(8,128)(2,1)S(1)} %get-tuple-element.55), channel_id=1, source_target_pairs={{0,2},{2,4},{4,6},{6,8},{8,10},{10,12},{12,14},{14,16},{16,18},{18... | collective-permute-start | bytes 92168 | tf_op jit(solution)/shard_map/ppermute | solution.py:19
  7.3 13.4 %collective-permute-start.1 = (bf16[15,1024]{1,0:T(8,128)(2,1)S(1)}, bf16[15,1024]{1,0:T(8,128)(2,1)S(1)}, u32[]{:S(2)}, u32[]{:S(2)}) collective-permute-start(bf16[15,1024]{1,0:T(8,128)(2,1)S(1)} %get-tuple-element.56), channel_id=1, source_target_pairs={{2,0},{4,2},{6,4},{8,6},{10,8},{12,10},{14,12},{16,14},{18,16},{20... | collective-permute-start | bytes 92168 | tf_op jit(solution)/shard_map/ppermute | solution.py:21
  15.4 5.0 %copy-start.6 = (f32[31,1024]{1,0:T(8,128)S(1)}, f32[31,1024]{1,0:T(8,128)}, u32[]{:S(2)}) copy-start(f32[31,1024]{1,0:T(8,128)} %param.9) | copy-start | bytes 380932
  15.4 24.3 %all-to-all-start = ((bf16[4,2,360,256]{3,2,1,0:T(8,128)(2,1)}), bf16[4,2,360,256]{3,2,1,0:T(8,128)(2,1)}, u32[]{:S(2)}, u32[]{:S(2)}) async-start(bf16[4,2,360,256]{3,2,1,0:T(8,128)(2,1)} %bitcast.101), calls=%async_computation | async-start | bytes 2949120 | tf_op jit(solution)/shard_map/all_to_all | solution.py:28
  20.4 7.3 %copy-start.7 = (f32[1,1024]{1,0:T(1,128)}, f32[1,1024]{1,0:T(1,128)S(1)}, u32[]{:S(2)}) copy-start(f32[1,1024]{1,0:T(1,128)S(1)} %get-tuple-element.75) | copy-start | bytes 12292
  20.4 7.3 %copy-start.8 = (f32[1,1024]{1,0:T(1,128)}, f32[1,1024]{1,0:T(1,128)S(1)}, u32[]{:S(2)}) copy-start(f32[1,1024]{1,0:T(1,128)S(1)} %get-tuple-element.76) | copy-start | bytes 12292
  20.5 7.3 %copy-start.9 = (f32[1,1024]{1,0:T(1,128)}, f32[1,1024]{1,0:T(1,128)S(1)}, u32[]{:S(2)}) copy-start(f32[1,1024]{1,0:T(1,128)S(1)} %get-tuple-element.77) | copy-start | bytes 12292
  20.5 7.3 %copy-start.10 = (f32[1,1024]{1,0:T(1,128)}, f32[1,1024]{1,0:T(1,128)S(1)}, u32[]{:S(2)}) copy-start(f32[1,1024]{1,0:T(1,128)S(1)} %get-tuple-element.78) | copy-start | bytes 12292
  20.5 7.3 %copy-start.11 = (f32[1,1024]{1,0:T(1,128)}, f32[1,1024]{1,0:T(1,128)S(1)}, u32[]{:S(2)}) copy-start(f32[1,1024]{1,0:T(1,128)S(1)} %get-tuple-element.79) | copy-start | bytes 12292
  20.5 7.3 %copy-start.12 = (f32[1,1024]{1,0:T(1,128)}, f32[1,1024]{1,0:T(1,128)S(1)}, u32[]{:S(2)}) copy-start(f32[1,1024]{1,0:T(1,128)S(1)} %get-tuple-element.80) | copy-start | bytes 12292
  20.5 7.3 %copy-start.13 = (f32[1,1024]{1,0:T(1,128)}, f32[1,1024]{1,0:T(1,128)S(1)}, u32[]{:S(2)}) copy-start(f32[1,1024]{1,0:T(1,128)S(1)} %get-tuple-element.81) | copy-start | bytes 12292
  20.6 7.3 %copy-start.14 = (f32[1,1024]{1,0:T(1,128)}, f32[1,1024]{1,0:T(1,128)S(1)}, u32[]{:S(2)}) copy-start(f32[1,1024]{1,0:T(1,128)S(1)} %get-tuple-element.82) | copy-start | bytes 12292
  20.6 7.3 %copy-start.15 = (f32[1,1024]{1,0:T(1,128)}, f32[1,1024]{1,0:T(1,128)S(1)}, u32[]{:S(2)}) copy-start(f32[1,1024]{1,0:T(1,128)S(1)} %get-tuple-element.83) | copy-start | bytes 12292
  20.6 7.3 %copy-start.16 = (f32[1,1024]{1,0:T(1,128)}, f32[1,1024]{1,0:T(1,128)S(1)}, u32[]{:S(2)}) copy-start(f32[1,1024]{1,0:T(1,128)S(1)} %get-tuple-element.84) | copy-start | bytes 12292
  20.6 7.3 %copy-start.17 = (f32[1,1024]{1,0:T(1,128)}, f32[1,1024]{1,0:T(1,128)S(1)}, u32[]{:S(2)}) copy-start(f32[1,1024]{1,0:T(1,128)S(1)} %get-tuple-element.85) | copy-start | bytes 12292
  20.6 7.3 %copy-start.18 = (f32[1,1024]{1,0:T(1,128)}, f32[1,1024]{1,0:T(1,128)S(1)}, u32[]{:S(2)}) copy-start(f32[1,1024]{1,0:T(1,128)S(1)} %get-tuple-element.86) | copy-start | bytes 12292
  20.6 7.3 %copy-start.19 = (f32[1,1024]{1,0:T(1,128)}, f32[1,1024]{1,0:T(1,128)S(1)}, u32[]{:S(2)}) copy-start(f32[1,1024]{1,0:T(1,128)S(1)} %get-tuple-element.87) | copy-start | bytes 12292
  20.6 7.3 %copy-start.20 = (f32[1,1024]{1,0:T(1,128)}, f32[1,1024]{1,0:T(1,128)S(1)}, u32[]{:S(2)}) copy-start(f32[1,1024]{1,0:T(1,128)S(1)} %get-tuple-element.88) | copy-start | bytes 12292
  20.6 7.3 %copy-start.21 = (f32[1,1024]{1,0:T(1,128)}, f32[1,1024]{1,0:T(1,128)S(1)}, u32[]{:S(2)}) copy-start(f32[1,1024]{1,0:T(1,128)S(1)} %get-tuple-element.89) | copy-start | bytes 12292
  27.9 5.3 %copy-start.22 = (f32[1024]{0:T(1024)S(1)}, f32[1024]{0:T(1024)}, u32[]{:S(2)}) copy-start(f32[1024]{0:T(1024)} %param.10) | copy-start | bytes 12292
  27.9 5.3 %copy-start.23 = (f32[1024]{0:T(1024)S(1)}, f32[1024]{0:T(1024)}, u32[]{:S(2)}) copy-start(f32[1024]{0:T(1024)} %param.11) | copy-start | bytes 12292
  39.7 2.7 %copy-start.4 = (bf16[360,1024]{1,0:T(8,128)(2,1)S(1)}, bf16[360,1024]{1,0:T(8,128)(2,1)}, u32[]{:S(2)}) copy-start(bf16[360,1024]{1,0:T(8,128)(2,1)} %multiply_convert_fusion.1) | copy-start | bytes 2211844
  44.3 55.3 %all-to-all-start.4 = ((bf16[4,360,1024]{2,1,0:T(8,128)(2,1)}), bf16[4,360,1024]{2,1,0:T(8,128)(2,1)}, u32[]{:S(2)}, u32[]{:S(2)}) async-start(bf16[4,360,1024]{2,1,0:T(8,128)(2,1)} %broadcast_in_dim.5), calls=%async_computation.4 | async-start | bytes 5898240 | tf_op jit(solution)/shard_map/all_to_all | solution.py:28
  48.9 43.2 %collective-permute-start.2 = (bf16[2,1440,256]{2,1,0:T(8,128)(2,1)}, bf16[2,1440,256]{2,1,0:T(8,128)(2,1)S(1)}, u32[]{:S(2)}, u32[]{:S(2)}) collective-permute-start(bf16[2,1440,256]{2,1,0:T(8,128)(2,1)} %bitcast.103), channel_id=1, source_target_pairs={{0,1},{1,0},{2,3},{3,2},{4,5},{5,4},{6,7},{7,6},{8,9},{9,8},{10,11... | collective-permute-start | bytes 4423688 | tf_op jit(solution)/shard_map/ppermute | solution.py:121
  49.0 9.0 %collective-permute-start.3 = (bf16[1024,256]{1,0:T(8,128)(2,1)}, bf16[1024,256]{1,0:T(8,128)(2,1)S(1)}, u32[]{:S(2)}, u32[]{:S(2)}) collective-permute-start(bf16[1024,256]{1,0:T(8,128)(2,1)} %param.12), channel_id=1, source_target_pairs={{0,0},{17,1},{8,8},{25,9},{16,16},{1,17},{24,24},{9,25},{2,2},{19,... | collective-permute-start | bytes 1572872 | tf_op jit(solution)/shard_map/ppermute | solution.py:76
  50.7 21.5 %collective-permute-start.4 = (bf16[1024,256]{1,0:T(8,128)(2,1)}, bf16[1024,256]{1,0:T(8,128)(2,1)S(1)}, u32[]{:S(2)}, u32[]{:S(2)}) collective-permute-start(bf16[1024,256]{1,0:T(8,128)(2,1)} %param.12), channel_id=1, source_target_pairs={{8,0},{25,1},{0,8},{17,9},{24,16},{9,17},{16,24},{1,25},{10,2},{27... | collective-permute-start | bytes 1572872 | tf_op jit(solution)/shard_map/ppermute | solution.py:76
  53.4 38.7 %collective-permute-start.5 = (bf16[1024,256]{1,0:T(8,128)(2,1)}, bf16[1024,256]{1,0:T(8,128)(2,1)S(1)}, u32[]{:S(2)}, u32[]{:S(2)}) collective-permute-start(bf16[1024,256]{1,0:T(8,128)(2,1)} %param.12), channel_id=1, source_target_pairs={{16,0},{1,1},{24,8},{9,9},{0,16},{17,17},{8,24},{25,25},{18,2},{3,... | collective-permute-start | bytes 1572872 | tf_op jit(solution)/shard_map/ppermute | solution.py:76
  57.8 34.2 %collective-permute-start.6 = (bf16[1024,256]{1,0:T(8,128)(2,1)}, bf16[1024,256]{1,0:T(8,128)(2,1)S(1)}, u32[]{:S(2)}, u32[]{:S(2)}) collective-permute-start(bf16[1024,256]{1,0:T(8,128)(2,1)} %param.12), channel_id=1, source_target_pairs={{24,0},{9,1},{16,8},{1,9},{8,16},{25,17},{0,24},{17,25},{26,2},{11... | collective-permute-start | bytes 1572872 | tf_op jit(solution)/shard_map/ppermute | solution.py:76
  92.0 1.2 copy-start.24
  99.5 39.5 %all-to-all-start.1 = ((bf16[4,360,1024]{2,1,0:T(8,128)(2,1)}), bf16[4,360,1024]{2,1,0:T(8,128)(2,1)}, u32[]{:S(2)}, u32[]{:S(2)}) async-start(bf16[4,360,1024]{2,1,0:T(8,128)(2,1)} %bitcast.102), calls=%async_computation.1 | async-start | bytes 5898240 | tf_op jit(solution)/shard_map/all_to_all | solution.py:28
  104.1 17.9 %copy-start.25 = (bf16[2,1440,256]{2,1,0:T(8,128)(2,1)S(1)}, bf16[2,1440,256]{2,1,0:T(8,128)(2,1)}, u32[]{:S(2)}) copy-start(bf16[2,1440,256]{2,1,0:T(8,128)(2,1)} %copy-done.24) | copy-start | bytes 4423684
  108.1 18.2 %copy-start.5 = (bf16[2,4,360,256]{3,2,1,0:T(8,128)(2,1)S(1)}, bf16[2,4,360,256]{3,2,1,0:T(8,128)(2,1)}, u32[]{:S(2)}) copy-start(bf16[2,4,360,256]{3,2,1,0:T(8,128)(2,1)} %copy.14) | copy-start | bytes 4423684
  108.1 61.0 %collective-permute-start.10 = (bf16[1024,256]{1,0:T(8,128)(2,1)}, bf16[1024,256]{1,0:T(8,128)(2,1)}, u32[]{:S(2)}, u32[]{:S(2)}) collective-permute-start(bf16[1024,256]{1,0:T(8,128)(2,1)} %convolution_convert_fusion.2), channel_id=1, source_target_pairs={{0,16},{1,1},{8,24},{9,9},{16,0},{17,17},{24,8},{25,25},{2,18},{3,... | collective-permute-start | bytes 1572872 | tf_op jit(solution)/shard_map/ppermute | solution.py:72
  125.7 48.1 %collective-permute-start.9 = (bf16[1024,256]{1,0:T(8,128)(2,1)}, bf16[1024,256]{1,0:T(8,128)(2,1)}, u32[]{:S(2)}, u32[]{:S(2)}) collective-permute-start(bf16[1024,256]{1,0:T(8,128)(2,1)} %convolution_convert_fusion.3), channel_id=1, source_target_pairs={{0,24},{1,9},{8,16},{9,1},{16,8},{17,25},{24,0},{25,17},{2,26},{3,... | collective-permute-start | bytes 1572872 | tf_op jit(solution)/shard_map/ppermute | solution.py:72
  129.9 43.9 %collective-permute-start.11 = (bf16[1024,256]{1,0:T(8,128)(2,1)}, bf16[1024,256]{1,0:T(8,128)(2,1)}, u32[]{:S(2)}, u32[]{:S(2)}) collective-permute-start(bf16[1024,256]{1,0:T(8,128)(2,1)} %convolution_convert_fusion.1), channel_id=1, source_target_pairs={{0,8},{1,25},{8,0},{9,17},{16,24},{17,9},{24,16},{25,1},{2,10},{3,... | collective-permute-start | bytes 1572872 | tf_op jit(solution)/shard_map/ppermute | solution.py:72
  133.6 40.2 %collective-permute-start.12 = (bf16[1024,256]{1,0:T(8,128)(2,1)}, bf16[1024,256]{1,0:T(8,128)(2,1)}, u32[]{:S(2)}, u32[]{:S(2)}) collective-permute-start(bf16[1024,256]{1,0:T(8,128)(2,1)} %convolution_convert_fusion), channel_id=1, source_target_pairs={{0,0},{1,17},{8,8},{9,25},{16,16},{17,1},{24,24},{25,9},{2,2},{3,1... | collective-permute-start | bytes 1572872 | tf_op jit(solution)/shard_map/ppermute | solution.py:72
  151.6 2.4 %copy-start = (f32[360,1024]{1,0:T(8,128)}, f32[360,1024]{1,0:T(8,128)S(1)}, u32[]{:S(2)}) copy-start(f32[360,1024]{1,0:T(8,128)S(1)} %get-tuple-element.47) | copy-start | bytes 4423684
  154.0 13.8 %copy-start.1 = (f32[360,1024]{1,0:T(8,128)S(1)}, f32[360,1024]{1,0:T(8,128)}, u32[]{:S(2)}) copy-start(f32[360,1024]{1,0:T(8,128)} %copy-done) | copy-start | bytes 4423684
  155.1 22.9 %all-to-all-start.2 = ((f32[16,3,1024]{2,1,0:T(4,128)}), f32[16,3,1024]{2,1,0:T(4,128)S(1)}, u32[]{:S(2)}, u32[]{:S(2)}) async-start(f32[16,3,1024]{2,1,0:T(4,128)} %reshape.41), calls=%async_computation.2 | async-start | bytes 524288 | tf_op jit(solution)/shard_map/all_to_all | solution.py:28
  167.8 17.4 %collective-permute-start.7 = (f32[15,1024]{1,0:T(8,128)S(1)}, f32[15,1024]{1,0:T(8,128)S(1)}, u32[]{:S(2)}, u32[]{:S(2)}) collective-permute-start(f32[15,1024]{1,0:T(8,128)S(1)} %get-tuple-element.53), channel_id=1, source_target_pairs={{2,0},{4,2},{6,4},{8,6},{10,8},{12,10},{14,12},{16,14},{18,16},{20... | collective-permute-start | bytes 184328 | tf_op jit(solution)/shard_map/ppermute | solution.py:21
  169.1 16.1 %copy-start.2 = (bf16[360,1024]{1,0:T(8,128)(2,1)S(1)}, bf16[360,1024]{1,0:T(8,128)(2,1)}, u32[]{:S(2)}) copy-start(bf16[360,1024]{1,0:T(8,128)(2,1)} %param.8) | copy-start | bytes 2211844
  169.1 16.1 %copy-start.3 = (bf16[360,1024]{1,0:T(8,128)(2,1)S(1)}, bf16[360,1024]{1,0:T(8,128)(2,1)}, u32[]{:S(2)}) copy-start(bf16[360,1024]{1,0:T(8,128)(2,1)} %param.7) | copy-start | bytes 2211844
  169.1 16.1 %collective-permute-start.8 = (f32[15,1024]{1,0:T(8,128)S(1)}, f32[15,1024]{1,0:T(8,128)S(1)}, u32[]{:S(2)}, u32[]{:S(2)}) collective-permute-start(f32[15,1024]{1,0:T(8,128)S(1)} %get-tuple-element.54), channel_id=1, source_target_pairs={{0,2},{2,4},{4,6},{6,8},{8,10},{10,12},{12,14},{14,16},{16,18},{18... | collective-permute-start | bytes 184328 | tf_op jit(solution)/shard_map/ppermute | solution.py:19
  178.8 16.5 %all-to-all-start.3 = ((f32[16,3,1024]{2,1,0:T(4,128)}), f32[16,3,1024]{2,1,0:T(4,128)S(1)}, u32[]{:S(2)}, u32[]{:S(2)}) async-start(f32[16,3,1024]{2,1,0:T(4,128)} %broadcast_in_dim.4), calls=%async_computation.3 | async-start | bytes 524288 | tf_op jit(solution)/shard_map/all_to_all | solution.py:28

commit v3 on v1

--- a/solution.py
+++ b/solution.py
@@ -1,6 +1,8 @@
 import jax
 import jax.numpy as jnp
 from jax import lax
+from jax.experimental import pallas as pl
+from jax.experimental.pallas import tpu as pltpu
 from jax.sharding import Mesh, PartitionSpec as P
 
 
@@ -58,6 +60,28 @@
     return lax.ppermute(block, axis, [(partner(i, step, count), i) for i in range(count)])
 
 
+def copy_block(places, source, target):
+    target[0] = source[...]
+
+
+def column_blocks(out_grad, places, cols):
+    rows = out_grad.shape[0]
+    if cols % 128:
+        return jnp.stack([lax.dynamic_slice_in_dim(out_grad, p * cols, cols, axis=1) for p in places])
+    count = len(places)
+    return pl.pallas_call(
+        copy_block,
+        grid_spec=pltpu.PrefetchScalarGridSpec(
+            num_scalar_prefetch=1,
+            grid=(count,),
+            in_specs=[pl.BlockSpec((rows, cols), lambda g, p: (0, p[g]))],
+            out_specs=pl.BlockSpec((1, rows, cols), lambda g, p: (g, 0, 0)),
+        ),
+        out_shape=jax.ShapeDtypeStruct((count, rows, cols), out_grad.dtype),
+        name="column_blocks",
+    )(jnp.stack(places), out_grad)
+
+
 def plane_columns(out_grad, cols):
     far, near, tp = (lax.axis_size(a) for a in ("far", "near", "tp"))
     rows = out_grad.shape[0]
@@ -65,12 +89,12 @@
     piece = far // tp if shared else far
     base = lax.axis_index("tp") * piece if shared else 0
     me = lax.axis_index("far")
-    blocks = []
-    for n in range(near):
-        for k in range(piece):
-            start = (partner(me, base + k, far) * near + n) * cols
-            blocks.append(lax.dynamic_slice_in_dim(out_grad, start, cols, axis=1))
-    blocks = jnp.stack(blocks).reshape(near, piece, rows, cols)
+    places = [
+        jnp.asarray(partner(me, base + k, far) * near + n, jnp.int32)
+        for n in range(near)
+        for k in range(piece)
+    ]
+    blocks = column_blocks(out_grad, places, cols).reshape(near, piece, rows, cols)
     got = exchange(blocks, "near")
     got = got.transpose(1, 0, 2, 3)
     if shared:

time: 256 us -> 250 us (0.977)
  local copies, waits for them, and re-layouts: 20.6 us -> 8.38 us
  Pallas kernels: 0 us -> 6.06 us
    unnamed x73 -> x66, local copies, waits for them, and re-layouts: 11.4 us -> 0.16 us
    pallas_call x0 -> x1, Pallas kernels: none -> 6.06 us  [column_blocks(): pl.pallas_call(copy_block, grid_spec=pltpu.PrefetchScalarGridSpec(num_sca...]
  transfers between devices with their start and end apart: 15 -> 15, of which waited for: 6 -> 6; matrix products, arithmetic and copies ran while one was open for 22% -> 18% of each run, Pallas kernels for 0% -> 2%
where the time goes in v3:
time: 250 us; the launch traced here: 249 us
  waiting for transfers between devices  105 us (42%)
  starting transfers between devices  56.3 us (23%)
  other arithmetic  34.4 us (14%)
  matrix products  22.9 us (9%)
  blocking collectives  14.6 us (6%)
  local copies, waits for them, and re-layouts  8.38 us (3%)
  Pallas kernels  6.06 us (2%)
    all_to_all x5, waiting for transfers between devices, exchange(): return lax.all_to_all(blocks, axis, split_axis=0, concat_axis=0)  68.8 us
    ppermute x3, waiting for transfers between devices, fetch(): lax.ppermute(block, axis, [(partner(i, step, count), i) for i in range(co...  35.8 us
    all_to_all x5, starting transfers between devices, exchange(): return lax.all_to_all(blocks, axis, split_axis=0, concat_axis=0)  25.3 us
    dot_general x4, matrix products, on_device(): lax.dot_general(act_near, grads[d], (((0,), (0,)), ((), ())), preferred_e...  16.1 us
    ppermute x3, starting transfers between devices, send(): lax.ppermute(block, axis, [(i, partner(i, step, count)) for i in range(co...  13.6 us
    ppermute x2, starting transfers between devices, padded_2(): lax.ppermute(tail, axis, [(i, (i + 1) % count) for i in range(ends)])  9.42 us
    convert_element_type x1, other arithmetic, on_device(): (mixed_grad * value_f * gate_sig * (1.0 - gate_sig)).astype(bf16)  8.84 us
    reduce_sum x2, other arithmetic, on_device(): jnp.sum(conv_grad * padded[k:k + rows], axis=0)  8.3 us
  transfers between devices with their start and end apart: 15, of which 6 were waited for; matrix products, arithmetic and copies ran while one was open for 18% of the time, Pallas kernels for 2%

profile of v3, /device:TPU:0, one launch (start us, length us, event | category | flops | bytes accessed | tf_op | source)
XLA Modules:
  0.0 248.5 jit_solution(14182978701428701792)
XLA Ops:
  0.6 1.8 fusion.7
  2.4 4.9 %collective-permute-start = (bf16[15,1024]{1,0:T(8,128)(2,1)S(1)}, bf16[15,1024]{1,0:T(8,128)(2,1)S(1)}, u32[]{:S(2)}, u32[]{:S(2)}) collective-permute-start(bf16[15,1024]{1,0:T(8,128)(2,1)S(1)} %get-tuple-element.55), channel_id=1, source_target_pairs={{0,2},{2,4},{4,6},{6,8},{8,10},{10,12},{12,14},{14,16},{16,18},{18... | collective-permute-start | bytes 92168 | tf_op jit(solution)/shard_map/ppermute | solution.py:19
  7.3 1.3 collective-permute-start.1
  8.6 0.6 stack.152.places
  9.2 6.1 %column_blocks.1 = bf16[8,360,256]{2,1,0:T(8,128)(2,1)} custom-call(s32[8]{0:T(128)} %stack.152.places, bf16[360,4096]{1,0:T(8,128)(2,1)} %source.1), custom_call_target="tpu_custom_call" | custom-call | tf_op jit(solution)/shard_map/column_blocks/pallas_call | solution.py:72
  15.3 5.0 %all-to-all-start = ((bf16[4,2,360,256]{3,2,1,0:T(8,128)(2,1)}), bf16[4,2,360,256]{3,2,1,0:T(8,128)(2,1)}, u32[]{:S(2)}, u32[]{:S(2)}) async-start(bf16[4,2,360,256]{3,2,1,0:T(8,128)(2,1)} %bitcast.104), calls=%async_computation | async-start | bytes 2949120 | tf_op jit(solution)/shard_map/all_to_all | solution.py:28
  20.8 6.9 %fusion.112 = (f32[360]{0:T(512)S(1)}, f32[360,1024]{1,0:T(8,128)S(1)}) fusion(f32[390,1024]{1,0:T(8,128)S(1)} %maximum_convert_fusion, f32[1024]{0:T(1024)S(1)} %bitcast.169, f32[1024]{0:T(1024)S(1)} %bitcast.171, f32[1024]{0:T(1024)S(1)} %bitcast.113, f32[1024]{0:T(1024)S(1)} %bitcast.115, f32[1024]{0:T(1024)S(1)} %bitcast.117, f32[1024]{0:T(1024)S(1)} %bitcast.119, ...), kind=kLoop, calls=%fused_computation.219 | loop fusion | flops 22855320 | bytes 47314336 | tf_op jit(solution)/shard_map/reduce_sum | solution.py:127
  27.9 2.5 psum.28
  30.4 0.3 multiply_reduce_fusion.33
  30.7 2.5 psum.29
  33.2 1.4 multiply_convert_fusion.1
  34.6 4.9 %all-to-all-done = bf16[4,2,360,256]{3,2,1,0:T(8,128)(2,1)} async-done(((bf16[4,2,360,256]{3,2,1,0:T(8,128)(2,1)}), bf16[4,2,360,256]{3,2,1,0:T(8,128)(2,1)}, u32[]{:S(2)}, u32[]{:S(2)}) %all-to-all-start) | async-done | bytes 1474592 | tf_op jit(solution)/shard_map/all_to_all | solution.py:28
  39.5 1.5 copy.14
  41.2 7.2 %all_to_all.30 = bf16[2,2,4,360,256]{4,3,2,1,0:T(8,128)(2,1)} all-to-all(bf16[2,2,4,360,256]{4,3,2,1,0:T(8,128)(2,1)S(1)} %broadcast_in_dim.6), channel_id=1, replica_groups=mesh['far'=4,'near'=4,'tp'=2] {'tp'}, dimensions={0} | all-to-all | bytes 5898240 | tf_op jit(solution)/shard_map/all_to_all | solution.py:28
  48.4 2.0 broadcast_in_dim.8
  50.4 4.6 %all-to-all-start.5 = ((bf16[4,360,1024]{2,1,0:T(8,128)(2,1)}), bf16[4,360,1024]{2,1,0:T(8,128)(2,1)}, u32[]{:S(2)}, u32[]{:S(2)}) async-start(bf16[4,360,1024]{2,1,0:T(8,128)(2,1)} %broadcast_in_dim.8), calls=%async_computation.5 | async-start | bytes 5898240 | tf_op jit(solution)/shard_map/all_to_all | solution.py:28
  55.1 2.8 %collective-permute-start.2 = (bf16[1024,256]{1,0:T(8,128)(2,1)}, bf16[1024,256]{1,0:T(8,128)(2,1)S(1)}, u32[]{:S(2)}, u32[]{:S(2)}) collective-permute-start(bf16[1024,256]{1,0:T(8,128)(2,1)} %param.12), channel_id=1, source_target_pairs={{8,0},{0,8},{24,16},{16,24},{9,1},{1,9},{25,17},{17,25},{10,2},{2,... | collective-permute-start | bytes 1572872 | tf_op jit(solution)/shard_map/ppermute | solution.py:60
  57.9 2.6 %collective-permute-start.3 = (bf16[1024,256]{1,0:T(8,128)(2,1)}, bf16[1024,256]{1,0:T(8,128)(2,1)S(1)}, u32[]{:S(2)}, u32[]{:S(2)}) collective-permute-start(bf16[1024,256]{1,0:T(8,128)(2,1)} %param.12), channel_id=1, source_target_pairs={{16,0},{24,8},{0,16},{8,24},{17,1},{25,9},{1,17},{9,25},{18,2},{26... | collective-permute-start | bytes 1572872 | tf_op jit(solution)/shard_map/ppermute | solution.py:60
  60.5 20.5 %collective-permute-done.2 = bf16[1024,256]{1,0:T(8,128)(2,1)S(1)} collective-permute-done((bf16[1024,256]{1,0:T(8,128)(2,1)}, bf16[1024,256]{1,0:T(8,128)(2,1)S(1)}, u32[]{:S(2)}, u32[]{:S(2)}) %collective-permute-start.2) | collective-permute-done | bytes 524320 | tf_op jit(solution)/shard_map/ppermute | solution.py:60
  80.9 15.3 %collective-permute-done.3 = bf16[1024,256]{1,0:T(8,128)(2,1)S(1)} collective-permute-done((bf16[1024,256]{1,0:T(8,128)(2,1)}, bf16[1024,256]{1,0:T(8,128)(2,1)S(1)}, u32[]{:S(2)}, u32[]{:S(2)}) %collective-permute-start.3) | collective-permute-done | bytes 524320 | tf_op jit(solution)/shard_map/ppermute | solution.py:60
  96.2 6.8 %bitcast_convert_fusion = bf16[1440,1024]{1,0:T(8,128)(2,1)} fusion(bf16[4,1440,256]{2,1,0:T(8,128)(2,1)} %bitcast.105, bf16[1,1024,256]{2,1,0:T(8,128)(2,1)S(1)} %bitcast.211, bf16[1,1024,256]{2,1,0:T(8,128)(2,1)S(1)} %bitcast.210, bf16[1,1024,256]{2,1,0:T(8,128)(2,1)S(1)} %bitcast.209, bf16[1,1024,256]{2,1,0:T(8,128)(2,1)} %bitcast.208), kind=kOutput, calls=%fused_computation.28 | convolution fusion | flops 3024519168 | bytes 7995392 | tf_op jit(solution)/shard_map/dot_general | solution.py:138
  103.1 4.9 %all-to-all-start.2 = ((bf16[4,360,1024]{2,1,0:T(8,128)(2,1)}), bf16[4,360,1024]{2,1,0:T(8,128)(2,1)}, u32[]{:S(2)}, u32[]{:S(2)}) async-start(bf16[4,360,1024]{2,1,0:T(8,128)(2,1)} %bitcast.110), calls=%async_computation.2 | async-start | bytes 5898240 | tf_op jit(solution)/shard_map/all_to_all | solution.py:28
  108.0 3.8 %convolution_convert_fusion.2 = bf16[1024,256]{1,0:T(8,128)(2,1)} fusion(bf16[1440,1024]{1,0:T(8,128)(2,1)} %bitcast.83, bf16[4,1440,256]{2,1,0:T(8,128)(2,1)} %bitcast.106), kind=kOutput, calls=%fused_computation.202 | convolution fusion | flops 755236864 | bytes 4210688 | tf_op jit(solution)/shard_map/dot_general | solution.py:147
  111.8 3.8 %convolution_convert_fusion.1 = bf16[1024,256]{1,0:T(8,128)(2,1)} fusion(bf16[1440,1024]{1,0:T(8,128)(2,1)} %bitcast.83, bf16[4,1440,256]{2,1,0:T(8,128)(2,1)} %bitcast.107), kind=kOutput, calls=%fused_computation.201 | convolution fusion | flops 755236864 | bytes 4210688 | tf_op jit(solution)/shard_map/dot_general | solution.py:147
  115.6 24.7 %all-to-all-done.2 = bf16[4,360,1024]{2,1,0:T(8,128)(2,1)} async-done(((bf16[4,360,1024]{2,1,0:T(8,128)(2,1)}), bf16[4,360,1024]{2,1,0:T(8,128)(2,1)}, u32[]{:S(2)}, u32[]{:S(2)}) %all-to-all-start.2) | async-done | bytes 2949152 | tf_op jit(solution)/shard_map/all_to_all | solution.py:28
  140.3 2.6 %convert_reduce_fusion = f32[360,1024]{1,0:T(8,128)S(1)} fusion(bf16[4,360,1024]{2,1,0:T(8,128)(2,1)} %all-to-all-done.2), kind=kLoop, calls=%fused_computation.29 | loop fusion | flops 2580480 | bytes 4423680 | tf_op jit(solution)/shard_map/reduce_sum | solution.py:142
  142.9 2.8 %multiply_reduce_fusion = (f32[1024]{0:T(1024)}, f32[360]{0:T(512)S(1)}, f32[360]{0:T(512)S(1)}, f32[1024]{0:T(1024)}, f32[360,1024]{1,0:T(8,128)}) fusion(f32[360,1024]{1,0:T(8,128)S(1)} %get-tuple-element.52, f32[360]{0:T(512)S(1)} %add_rsqrt_fusion, f32[360]{0:T(512)S(1)} %broadcast_multiply_fusion.1, f32[1024]{0:T(1024)S(1)} %copy-done.25, ...), kind=kLoop, calls=%fused_computation.157 | loop fusion | flops 7001392 | bytes 4445824 | tf_op jit(solution)/shard_map/reduce_sum | solution.py:166
  145.7 2.4 all-reduce.1
  148.2 5.9 %multiply_reduce_fusion.1 = (f32[1024]{0:T(1024)S(1)}, f32[1024]{0:T(1024)S(1)}, f32[1024]{0:T(1024)S(1)}, f32[1024]{0:T(1024)S(1)}, f32[1024]{0:T(1024)S(1)}, /...) fusion(f32[390,1024]{1,0:T(8,128)S(1)} %maximum_convert_fusion,, ...), kind=kLoop, calls=%fused_computation.158 | loop fusion | flops 16201728 | bytes 31049344 | tf_op jit(solution)/shard_map/reduce_sum | solution.py:165
  154.1 2.4 multiply_reduce_fusion.2
  156.5 0.6 fusion.113
  157.1 1.3 collective-permute-start.5
  158.5 4.5 %collective-permute-start.6 = (f32[15,1024]{1,0:T(8,128)S(1)}, f32[15,1024]{1,0:T(8,128)S(1)}, u32[]{:S(2)}, u32[]{:S(2)}) collective-permute-start(f32[15,1024]{1,0:T(8,128)S(1)} %get-tuple-element.54), channel_id=1, source_target_pairs={{0,2},{2,4},{4,6},{6,8},{8,10},{10,12},{12,14},{14,16},{16,18},{18... | collective-permute-start | bytes 184328 | tf_op jit(solution)/shard_map/ppermute | solution.py:19
  163.0 3.9 %convolution_convert_fusion = bf16[1024,256]{1,0:T(8,128)(2,1)} fusion(bf16[1440,1024]{1,0:T(8,128)(2,1)} %bitcast.83, bf16[4,1440,256]{2,1,0:T(8,128)(2,1)} %bitcast.108), kind=kOutput, calls=%fused_computation.200 | convolution fusion | flops 755236864 | bytes 4210688 | tf_op jit(solution)/shard_map/dot_general | solution.py:147
  167.0 13.0 %collective-permute-start.7 = (bf16[1024,256]{1,0:T(8,128)(2,1)}, bf16[1024,256]{1,0:T(8,128)(2,1)}, u32[]{:S(2)}, u32[]{:S(2)}) collective-permute-start(bf16[1024,256]{1,0:T(8,128)(2,1)} %convolution_convert_fusion.2), channel_id=1, source_target_pairs={{0,24},{8,16},{16,8},{24,0},{1,25},{9,17},{17,9},{25,1},{2,26},{10... | collective-permute-start | bytes 1572872 | tf_op jit(solution)/shard_map/ppermute | solution.py:55
  180.2 0.4 collective-permute-start.9
  180.6 0.3 stack.191
  180.9 0.8 reshape.42
  181.7 6.7 %all-to-all-start.3 = ((f32[16,3,1024]{2,1,0:T(4,128)}), f32[16,3,1024]{2,1,0:T(4,128)S(1)}, u32[]{:S(2)}, u32[]{:S(2)}) async-start(f32[16,3,1024]{2,1,0:T(4,128)} %reshape.42), calls=%async_computation.3 | async-start | bytes 524288 | tf_op jit(solution)/shard_map/all_to_all | solution.py:28
  188.4 8.8 %fusion.10 = (bf16[360,1024]{1,0:T(8,128)(2,1)}, f32[360,1024]{1,0:T(8,128)S(1)}) fusion(bf16[360,1024]{1,0:T(8,128)(2,1)S(1)} %copy-done.3, bf16[360,1024]{1,0:T(8,128)(2,1)S(1)} %copy-done.2, f32[360,1024]{1,0:T(8,128)S(1)} %copy-done.1, f32[15,1024]{1,0:T(8,128)S(1)} %collective-permute-done.6, f32[1024]{0:T(1024)} %bitcast.170, f32[1024]{0:T(1024)} %bitcast.172, ...), kind=kLoop, calls=%fused_computation.42 | loop fusion | flops 37232640 | bytes 5410816 | tf_op jit(solution)/shard_map/convert_element_type | solution.py:173
  197.3 1.3 multiply_convert_fusion
  198.5 34.1 %all-to-all-done.3 = f32[16,3,1024]{2,1,0:T(4,128)S(1)} async-done(((f32[16,3,1024]{2,1,0:T(4,128)}), f32[16,3,1024]{2,1,0:T(4,128)S(1)}, u32[]{:S(2)}, u32[]{:S(2)}) %all-to-all-start.3) | async-done | bytes 196640 | tf_op jit(solution)/shard_map/all_to_all | solution.py:28
  232.7 0.7 broadcast_in_dim.7
  233.4 4.2 %all-to-all-start.4 = ((f32[16,3,1024]{2,1,0:T(4,128)}), f32[16,3,1024]{2,1,0:T(4,128)S(1)}, u32[]{:S(2)}, u32[]{:S(2)}) async-start(f32[16,3,1024]{2,1,0:T(4,128)} %broadcast_in_dim.7), calls=%async_computation.4 | async-start | bytes 524288 | tf_op jit(solution)/shard_map/all_to_all | solution.py:28
  237.6 4.5 %add_add_fusion = f32[1024,256]{1,0:T(8,128)} fusion(bf16[1024,256]{1,0:T(8,128)(2,1)} %collective-permute-done.9, bf16[1024,256]{1,0:T(8,128)(2,1)} %collective-permute-done.8, bf16[1024,256]{1,0:T(8,128)(2,1)} %collective-permute-done.7, bf16[1440,1024]{1,0:T(8,128)(2,1)} %bitcast.83, bf16[4,1440,256]{2,1,0:T(8,128)(2,1)} %bitcast.109), kind=kOutput, calls=%fused_computation.204 | convolution fusion | flops 756547584 | bytes 6307840 | tf_op jit(solution)/shard_map/dot_general | solution.py:147
  242.1 5.1 %all-to-all-done.4 = f32[16,3,1024]{2,1,0:T(4,128)S(1)} async-done(((f32[16,3,1024]{2,1,0:T(4,128)}), f32[16,3,1024]{2,1,0:T(4,128)S(1)}, u32[]{:S(2)}, u32[]{:S(2)}) %all-to-all-start.4) | async-done | bytes 196640 | tf_op jit(solution)/shard_map/all_to_all | solution.py:28
  247.3 0.7 slice.604
  247.9 0.6 fusion.115
  (89 shorter events, 1.1 us)
Async XLA Ops:
  2.4 18.2 %collective-permute-start = (bf16[15,1024]{1,0:T(8,128)(2,1)S(1)}, bf16[15,1024]{1,0:T(8,128)(2,1)S(1)}, u32[]{:S(2)}, u32[]{:S(2)}) collective-permute-start(bf16[15,1024]{1,0:T(8,128)(2,1)S(1)} %get-tuple-element.55), channel_id=1, source_target_pairs={{0,2},{2,4},{4,6},{6,8},{8,10},{10,12},{12,14},{14,16},{16,18},{18... | collective-permute-start | bytes 92168 | tf_op jit(solution)/shard_map/ppermute | solution.py:19
  7.3 13.3 %collective-permute-start.1 = (bf16[15,1024]{1,0:T(8,128)(2,1)S(1)}, bf16[15,1024]{1,0:T(8,128)(2,1)S(1)}, u32[]{:S(2)}, u32[]{:S(2)}) collective-permute-start(bf16[15,1024]{1,0:T(8,128)(2,1)S(1)} %get-tuple-element.56), channel_id=1, source_target_pairs={{2,0},{4,2},{6,4},{8,6},{10,8},{12,10},{14,12},{16,14},{18,16},{20... | collective-permute-start | bytes 92168 | tf_op jit(solution)/shard_map/ppermute | solution.py:21
  15.3 5.0 %copy-start.5 = (f32[31,1024]{1,0:T(8,128)S(1)}, f32[31,1024]{1,0:T(8,128)}, u32[]{:S(2)}) copy-start(f32[31,1024]{1,0:T(8,128)} %param.9) | copy-start | bytes 380932
  15.3 24.2 %all-to-all-start = ((bf16[4,2,360,256]{3,2,1,0:T(8,128)(2,1)}), bf16[4,2,360,256]{3,2,1,0:T(8,128)(2,1)}, u32[]{:S(2)}, u32[]{:S(2)}) async-start(bf16[4,2,360,256]{3,2,1,0:T(8,128)(2,1)} %bitcast.104), calls=%async_computation | async-start | bytes 2949120 | tf_op jit(solution)/shard_map/all_to_all | solution.py:28
  20.4 7.4 %copy-start.6 = (f32[1,1024]{1,0:T(1,128)}, f32[1,1024]{1,0:T(1,128)S(1)}, u32[]{:S(2)}) copy-start(f32[1,1024]{1,0:T(1,128)S(1)} %get-tuple-element.71) | copy-start | bytes 12292
  20.4 7.4 %copy-start.7 = (f32[1,1024]{1,0:T(1,128)}, f32[1,1024]{1,0:T(1,128)S(1)}, u32[]{:S(2)}) copy-start(f32[1,1024]{1,0:T(1,128)S(1)} %get-tuple-element.72) | copy-start | bytes 12292
  20.4 7.4 %copy-start.8 = (f32[1,1024]{1,0:T(1,128)}, f32[1,1024]{1,0:T(1,128)S(1)}, u32[]{:S(2)}) copy-start(f32[1,1024]{1,0:T(1,128)S(1)} %get-tuple-element.73) | copy-start | bytes 12292
  20.4 7.4 %copy-start.9 = (f32[1,1024]{1,0:T(1,128)}, f32[1,1024]{1,0:T(1,128)S(1)}, u32[]{:S(2)}) copy-start(f32[1,1024]{1,0:T(1,128)S(1)} %get-tuple-element.74) | copy-start | bytes 12292
  20.4 7.4 %copy-start.10 = (f32[1,1024]{1,0:T(1,128)}, f32[1,1024]{1,0:T(1,128)S(1)}, u32[]{:S(2)}) copy-start(f32[1,1024]{1,0:T(1,128)S(1)} %get-tuple-element.75) | copy-start | bytes 12292
  20.4 7.4 %copy-start.11 = (f32[1,1024]{1,0:T(1,128)}, f32[1,1024]{1,0:T(1,128)S(1)}, u32[]{:S(2)}) copy-start(f32[1,1024]{1,0:T(1,128)S(1)} %get-tuple-element.76) | copy-start | bytes 12292
  20.4 7.4 %copy-start.12 = (f32[1,1024]{1,0:T(1,128)}, f32[1,1024]{1,0:T(1,128)S(1)}, u32[]{:S(2)}) copy-start(f32[1,1024]{1,0:T(1,128)S(1)} %get-tuple-element.77) | copy-start | bytes 12292
  20.5 7.3 %copy-start.13 = (f32[1,1024]{1,0:T(1,128)}, f32[1,1024]{1,0:T(1,128)S(1)}, u32[]{:S(2)}) copy-start(f32[1,1024]{1,0:T(1,128)S(1)} %get-tuple-element.78) | copy-start | bytes 12292
  20.5 7.3 %copy-start.14 = (f32[1,1024]{1,0:T(1,128)}, f32[1,1024]{1,0:T(1,128)S(1)}, u32[]{:S(2)}) copy-start(f32[1,1024]{1,0:T(1,128)S(1)} %get-tuple-element.79) | copy-start | bytes 12292
  20.5 7.3 %copy-start.15 = (f32[1,1024]{1,0:T(1,128)}, f32[1,1024]{1,0:T(1,128)S(1)}, u32[]{:S(2)}) copy-start(f32[1,1024]{1,0:T(1,128)S(1)} %get-tuple-element.80) | copy-start | bytes 12292
  20.5 7.3 %copy-start.16 = (f32[1,1024]{1,0:T(1,128)}, f32[1,1024]{1,0:T(1,128)S(1)}, u32[]{:S(2)}) copy-start(f32[1,1024]{1,0:T(1,128)S(1)} %get-tuple-element.81) | copy-start | bytes 12292
  20.5 7.3 %copy-start.17 = (f32[1,1024]{1,0:T(1,128)}, f32[1,1024]{1,0:T(1,128)S(1)}, u32[]{:S(2)}) copy-start(f32[1,1024]{1,0:T(1,128)S(1)} %get-tuple-element.82) | copy-start | bytes 12292
  20.5 7.3 %copy-start.18 = (f32[1,1024]{1,0:T(1,128)}, f32[1,1024]{1,0:T(1,128)S(1)}, u32[]{:S(2)}) copy-start(f32[1,1024]{1,0:T(1,128)S(1)} %get-tuple-element.83) | copy-start | bytes 12292
  20.5 7.3 %copy-start.19 = (f32[1,1024]{1,0:T(1,128)}, f32[1,1024]{1,0:T(1,128)S(1)}, u32[]{:S(2)}) copy-start(f32[1,1024]{1,0:T(1,128)S(1)} %get-tuple-element.84) | copy-start | bytes 12292
  20.5 7.3 %copy-start.20 = (f32[1,1024]{1,0:T(1,128)}, f32[1,1024]{1,0:T(1,128)S(1)}, u32[]{:S(2)}) copy-start(f32[1,1024]{1,0:T(1,128)S(1)} %get-tuple-element.85) | copy-start | bytes 12292
  20.6 7.3 %copy-start.21 = (f32[1,1024]{1,0:T(1,128)}, f32[1,1024]{1,0:T(1,128)S(1)}, u32[]{:S(2)}) copy-start(f32[1,1024]{1,0:T(1,128)S(1)} %get-tuple-element.86) | copy-start | bytes 12292
  20.6 7.3 %copy-start.22 = (f32[1,1024]{1,0:T(1,128)}, f32[1,1024]{1,0:T(1,128)S(1)}, u32[]{:S(2)}) copy-start(f32[1,1024]{1,0:T(1,128)S(1)} %get-tuple-element.87) | copy-start | bytes 12292
  20.6 7.3 %copy-start.23 = (f32[1,1024]{1,0:T(1,128)}, f32[1,1024]{1,0:T(1,128)S(1)}, u32[]{:S(2)}) copy-start(f32[1,1024]{1,0:T(1,128)S(1)} %get-tuple-element.88) | copy-start | bytes 12292
  20.6 7.3 %copy-start.24 = (f32[1,1024]{1,0:T(1,128)}, f32[1,1024]{1,0:T(1,128)S(1)}, u32[]{:S(2)}) copy-start(f32[1,1024]{1,0:T(1,128)S(1)} %get-tuple-element.89) | copy-start | bytes 12292
  27.9 5.3 %copy-start.25 = (f32[1024]{0:T(1024)S(1)}, f32[1024]{0:T(1024)}, u32[]{:S(2)}) copy-start(f32[1024]{0:T(1024)} %param.10) | copy-start | bytes 12292
  27.9 5.3 %copy-start.30 = (f32[1024]{0:T(1024)S(1)}, f32[1024]{0:T(1024)}, u32[]{:S(2)}) copy-start(f32[1024]{0:T(1024)} %param.11) | copy-start | bytes 12292
  41.2 7.2 %copy-start.4 = (bf16[360,1024]{1,0:T(8,128)(2,1)S(1)}, bf16[360,1024]{1,0:T(8,128)(2,1)}, u32[]{:S(2)}) copy-start(bf16[360,1024]{1,0:T(8,128)(2,1)} %multiply_convert_fusion.1) | copy-start | bytes 2211844
  50.4 52.6 %all-to-all-start.5 = ((bf16[4,360,1024]{2,1,0:T(8,128)(2,1)}), bf16[4,360,1024]{2,1,0:T(8,128)(2,1)}, u32[]{:S(2)}, u32[]{:S(2)}) async-start(bf16[4,360,1024]{2,1,0:T(8,128)(2,1)} %broadcast_in_dim.8), calls=%async_computation.5 | async-start | bytes 5898240 | tf_op jit(solution)/shard_map/all_to_all | solution.py:28
  55.1 25.9 %collective-permute-start.2 = (bf16[1024,256]{1,0:T(8,128)(2,1)}, bf16[1024,256]{1,0:T(8,128)(2,1)S(1)}, u32[]{:S(2)}, u32[]{:S(2)}) collective-permute-start(bf16[1024,256]{1,0:T(8,128)(2,1)} %param.12), channel_id=1, source_target_pairs={{8,0},{0,8},{24,16},{16,24},{9,1},{1,9},{25,17},{17,25},{10,2},{2,... | collective-permute-start | bytes 1572872 | tf_op jit(solution)/shard_map/ppermute | solution.py:60
  57.9 38.4 %collective-permute-start.3 = (bf16[1024,256]{1,0:T(8,128)(2,1)}, bf16[1024,256]{1,0:T(8,128)(2,1)S(1)}, u32[]{:S(2)}, u32[]{:S(2)}) collective-permute-start(bf16[1024,256]{1,0:T(8,128)(2,1)} %param.12), channel_id=1, source_target_pairs={{16,0},{24,8},{0,16},{8,24},{17,1},{25,9},{1,17},{9,25},{18,2},{26... | collective-permute-start | bytes 1572872 | tf_op jit(solution)/shard_map/ppermute | solution.py:60
  60.4 35.8 %collective-permute-start.4 = (bf16[1024,256]{1,0:T(8,128)(2,1)}, bf16[1024,256]{1,0:T(8,128)(2,1)S(1)}, u32[]{:S(2)}, u32[]{:S(2)}) collective-permute-start(bf16[1024,256]{1,0:T(8,128)(2,1)} %param.12), channel_id=1, source_target_pairs={{24,0},{16,8},{8,16},{0,24},{25,1},{17,9},{9,17},{1,25},{26,2},{18... | collective-permute-start | bytes 1572872 | tf_op jit(solution)/shard_map/ppermute | solution.py:60
  103.1 37.3 %all-to-all-start.2 = ((bf16[4,360,1024]{2,1,0:T(8,128)(2,1)}), bf16[4,360,1024]{2,1,0:T(8,128)(2,1)}, u32[]{:S(2)}, u32[]{:S(2)}) async-start(bf16[4,360,1024]{2,1,0:T(8,128)(2,1)} %bitcast.110), calls=%async_computation.2 | async-start | bytes 5898240 | tf_op jit(solution)/shard_map/all_to_all | solution.py:28
  154.1 2.4 copy-start
  157.1 31.3 %collective-permute-start.5 = (f32[15,1024]{1,0:T(8,128)}, f32[15,1024]{1,0:T(8,128)S(1)}, u32[]{:S(2)}, u32[]{:S(2)}) collective-permute-start(f32[15,1024]{1,0:T(8,128)} %get-tuple-element.53), channel_id=1, source_target_pairs={{2,0},{4,2},{6,4},{8,6},{10,8},{12,10},{14,12},{16,14},{18,16},{20... | collective-permute-start | bytes 184328 | tf_op jit(solution)/shard_map/ppermute | solution.py:21
  158.4 22.2 %copy-start.26 = (f32[1024]{0:T(1024)S(1)}, f32[1024]{0:T(1024)}, u32[]{:S(2)}) copy-start(f32[1024]{0:T(1024)} %get-tuple-element.24) | copy-start | bytes 12292
  158.4 22.2 %copy-start.27 = (f32[1024]{0:T(1024)S(1)}, f32[1024]{0:T(1024)}, u32[]{:S(2)}) copy-start(f32[1024]{0:T(1024)} %get-tuple-element.25) | copy-start | bytes 12292
  158.4 22.2 %copy-start.28 = (f32[1024]{0:T(1024)S(1)}, f32[1024]{0:T(1024)}, u32[]{:S(2)}) copy-start(f32[1024]{0:T(1024)} %get-tuple-element.26) | copy-start | bytes 12292
  158.4 22.2 %copy-start.29 = (f32[1024]{0:T(1024)S(1)}, f32[1024]{0:T(1024)}, u32[]{:S(2)}) copy-start(f32[1024]{0:T(1024)} %get-tuple-element.27) | copy-start | bytes 12292
  158.4 22.2 %copy-start.31 = (f32[1024]{0:T(1024)S(1)}, f32[1024]{0:T(1024)}, u32[]{:S(2)}) copy-start(f32[1024]{0:T(1024)} %get-tuple-element.41) | copy-start | bytes 12292
  158.5 22.2 %copy-start.32 = (f32[1024]{0:T(1024)S(1)}, f32[1024]{0:T(1024)}, u32[]{:S(2)}) copy-start(f32[1024]{0:T(1024)} %get-tuple-element.44) | copy-start | bytes 12292
  158.5 29.9 %collective-permute-start.6 = (f32[15,1024]{1,0:T(8,128)S(1)}, f32[15,1024]{1,0:T(8,128)S(1)}, u32[]{:S(2)}, u32[]{:S(2)}) collective-permute-start(f32[15,1024]{1,0:T(8,128)S(1)} %get-tuple-element.54), channel_id=1, source_target_pairs={{0,2},{2,4},{4,6},{6,8},{8,10},{10,12},{12,14},{14,16},{16,18},{18... | collective-permute-start | bytes 184328 | tf_op jit(solution)/shard_map/ppermute | solution.py:19
  163.0 25.4 %copy-start.2 = (bf16[360,1024]{1,0:T(8,128)(2,1)S(1)}, bf16[360,1024]{1,0:T(8,128)(2,1)}, u32[]{:S(2)}) copy-start(bf16[360,1024]{1,0:T(8,128)(2,1)} %param.8) | copy-start | bytes 2211844
  163.0 25.4 %copy-start.3 = (bf16[360,1024]{1,0:T(8,128)(2,1)S(1)}, bf16[360,1024]{1,0:T(8,128)(2,1)}, u32[]{:S(2)}) copy-start(bf16[360,1024]{1,0:T(8,128)(2,1)} %param.7) | copy-start | bytes 2211844
  167.0 21.4 %copy-start.1 = (f32[360,1024]{1,0:T(8,128)S(1)}, f32[360,1024]{1,0:T(8,128)}, u32[]{:S(2)}) copy-start(f32[360,1024]{1,0:T(8,128)} %copy-done) | copy-start | bytes 4423684
  167.0 70.6 %collective-permute-start.7 = (bf16[1024,256]{1,0:T(8,128)(2,1)}, bf16[1024,256]{1,0:T(8,128)(2,1)}, u32[]{:S(2)}, u32[]{:S(2)}) collective-permute-start(bf16[1024,256]{1,0:T(8,128)(2,1)} %convolution_convert_fusion.2), channel_id=1, source_target_pairs={{0,24},{8,16},{16,8},{24,0},{1,25},{9,17},{17,9},{25,1},{2,26},{10... | collective-permute-start | bytes 1572872 | tf_op jit(solution)/shard_map/ppermute | solution.py:55
  180.0 57.6 %collective-permute-start.8 = (bf16[1024,256]{1,0:T(8,128)(2,1)}, bf16[1024,256]{1,0:T(8,128)(2,1)}, u32[]{:S(2)}, u32[]{:S(2)}) collective-permute-start(bf16[1024,256]{1,0:T(8,128)(2,1)} %convolution_convert_fusion.1), channel_id=1, source_target_pairs={{0,16},{8,24},{16,0},{24,8},{1,17},{9,25},{17,1},{25,9},{2,18},{10... | collective-permute-start | bytes 1572872 | tf_op jit(solution)/shard_map/ppermute | solution.py:55
  180.2 57.4 %collective-permute-start.9 = (bf16[1024,256]{1,0:T(8,128)(2,1)}, bf16[1024,256]{1,0:T(8,128)(2,1)}, u32[]{:S(2)}, u32[]{:S(2)}) collective-permute-start(bf16[1024,256]{1,0:T(8,128)(2,1)} %convolution_convert_fusion), channel_id=1, source_target_pairs={{0,8},{8,0},{16,24},{24,16},{1,9},{9,1},{17,25},{25,17},{2,10},{10... | collective-permute-start | bytes 1572872 | tf_op jit(solution)/shard_map/ppermute | solution.py:55
  181.7 50.9 %all-to-all-start.3 = ((f32[16,3,1024]{2,1,0:T(4,128)}), f32[16,3,1024]{2,1,0:T(4,128)S(1)}, u32[]{:S(2)}, u32[]{:S(2)}) async-start(f32[16,3,1024]{2,1,0:T(4,128)} %reshape.42), calls=%async_computation.3 | async-start | bytes 524288 | tf_op jit(solution)/shard_map/all_to_all | solution.py:28
  233.4 13.7 %all-to-all-start.4 = ((f32[16,3,1024]{2,1,0:T(4,128)}), f32[16,3,1024]{2,1,0:T(4,128)S(1)}, u32[]{:S(2)}, u32[]{:S(2)}) async-start(f32[16,3,1024]{2,1,0:T(4,128)} %broadcast_in_dim.7), calls=%async_computation.4 | async-start | bytes 524288 | tf_op jit(solution)/shard_map/all_to_all | solution.py:28
